TPU v7x, 32 devices: a whole 2x2x4 slice. The times are simulated.
32 devices in a mesh: ep: 8 (over z, y), tp: 4 (over x, core).
Axes of the slice: x: 2, y: 2, z: 4, core: 2. Of those that a mesh axis runs over, the one named last changes fastest.
Arguments:
- queries: bfloat16 [1024, 512], P('ep', 'tp'), may hold values from -8 to 8
- key_cache: bfloat16 [4, 64, 1024], P('tp', None, 'ep'), may hold values from -4.5 to 4.5
- value_cache: bfloat16 [4, 64, 1024], P('tp', None, 'ep'), may hold values from -6 to 6
- cum_gate: float32 [4, 1024], P('tp'), may hold values from -256 to 0, as said below
- out_weight: bfloat16 [512, 2048], replicated, may hold values from -1 to 1
- routed_input: bfloat16 [2048, 2048], P('ep'), may hold values from -6 to 6
- norm_gain: bfloat16 [2048], replicated, may hold values from 0.099609375 to 1.8984375
- routes: int32 [2048, 2], P('ep'), may hold values from 0 to 7, all different within a row; in each aligned block of 64 rows (0 to 63, 64 to 127, ...) at most 24 rows name the same one
- route_weight: float32 [2048, 2], P('ep'), may hold values from 0.2 to 1
- expert_gate: bfloat16 [8, 2048, 1024], P('ep', None, 'tp'), may hold values from -0.125 to 0.125
- expert_up: bfloat16 [8, 2048, 1024], P('ep', None, 'tp'), may hold values from -0.125 to 0.125
- expert_down: bfloat16 [8, 1024, 2048], P('ep', 'tp'), may hold values from -0.1875 to 0.1875
Outputs:
- mixed_out: bfloat16 [1024, 2048], P(('ep', 'tp'))
- expert_out: bfloat16 [2048, 2048], P(('ep', 'tp'))
Inputs may be any that keep to these rules, and one draw needn't show every extreme that they name: `cum_gate`: Non-increasing along positions in every head. `routes`: each row names 2 different experts. In each aligned block of 64 rows (the rows of one device) no expert is named by more than 24 rows, a bound that some block reaches.
All inputs are finite; a program needn't handle non-finite values.
Results may differ from a plain program's by a relative error of at most 0.012.
Values may be sent and summed in bfloat16 or wider, within the bound.
A program may use at most 64 MiB of HBM per device.

v0:
```python
import functools

import jax
import jax.numpy as jnp
from jax import lax
from jax.experimental import pallas as pl
from jax.experimental.pallas import tpu as pltpu
from jax.sharding import PartitionSpec as P

MESH = pl.DeviceIdType.MESH


def fused_kernel(
    n,
    tpn,
    cap,
    q_any,
    gate_any,
    gain_any,
    routes_any,
    rw_any,
    k_any,
    v_any,
    ow_any,
    x_any,
    wg_any,
    wu_any,
    wd_any,
    mixed_ref,
    out_ref,
    q_ref,
    gate_ref,
    gain_ref,
    routes_ref,
    rw_ref,
    xbuf,
    wgv,
    wuv,
    wdv,
    owv,
    kv,
    att,
    attr,
    sel,
    sbuf,
    sbuf2,
    recv,
    part,
    r1,
    s2,
    r2,
    s3,
    rbuf,
    lsem,
    kvs,
    kvr,
    ats,
    atr,
    a_s,
    a_r,
    bx_s,
    bx_r,
    bc_s,
    bc_r,
    c_s,
    c_r,
    r1_s,
    r1_r,
    r2_s,
    r2_r,
    r3_s,
    r3_r,
):
    e = lax.axis_index("ep")
    t = lax.axis_index("tp")
    partner = t + 1 - 2 * lax.rem(t, 2)
    peer = lax.rem(t + 2, tpn)
    opp = lax.rem(partner + 2, tpn)
    mate = e + 1 - 2 * lax.rem(e, 2)
    half = n // 2
    _, own_rows, width = xbuf.shape
    wide = width // 2
    head = k_any.shape[1]
    seq = q_ref.shape[0]

    barrier = pltpu.get_barrier_semaphore()
    for s in range(1, n):
        pl.semaphore_signal(
            barrier, inc=1, device_id={"ep": lax.rem(e + s, n), "tp": t}, device_id_type=MESH
        )
    for s in range(1, tpn):
        pl.semaphore_signal(
            barrier, inc=1, device_id={"ep": e, "tp": lax.rem(t + s, tpn)}, device_id_type=MESH
        )

    def load_x(j):
        at = lax.rem(t + j, tpn) * own_rows
        return pltpu.make_async_copy(x_any.at[pl.ds(at, own_rows)], xbuf.at[j], lsem.at[12 + j])

    load_k = pltpu.make_async_copy(k_any.at[0], kv.at[e, pl.ds(0, head)], lsem.at[1])
    load_v = pltpu.make_async_copy(v_any.at[0], kv.at[e, pl.ds(head, head)], lsem.at[2])
    load_g = pltpu.make_async_copy(wg_any.at[0], wgv, lsem.at[3])
    load_u = pltpu.make_async_copy(wu_any.at[0], wuv, lsem.at[4])
    load_d = pltpu.make_async_copy(wd_any.at[0], wdv, lsem.at[5])
    load_o = pltpu.make_async_copy(ow_any, owv, lsem.at[6])
    load_q = pltpu.make_async_copy(q_any, q_ref, lsem.at[8])
    load_c = pltpu.make_async_copy(gate_any, gate_ref, lsem.at[9])
    load_n = pltpu.make_async_copy(gain_any, gain_ref, lsem.at[10])
    load_r = pltpu.make_async_copy(routes_any, routes_ref, lsem.at[11])
    load_w = pltpu.make_async_copy(rw_any, rw_ref, lsem.at[0])
    load_k.start()
    load_v.start()
    load_x(0).start()
    load_r.start()
    load_n.start()
    load_w.start()
    load_q.start()
    load_c.start()
    for j in range(1, tpn):
        load_x(j).start()
    load_g.start()
    load_u.start()
    load_d.start()
    load_o.start()

    def remote(src, dst, ssem, rsem, ep, tp):
        return pltpu.make_async_remote_copy(
            src_ref=src,
            dst_ref=dst,
            send_sem=ssem,
            recv_sem=rsem,
            device_id={"ep": ep, "tp": tp},
            device_id_type=MESH,
        )

    def kv_far(s):
        return remote(kv.at[e], kv.at[e], kvs.at[s], kvr.at[s], lax.rem(e + 2 * s, n), t)

    def kv_far_in(s):
        src = lax.rem(e - 2 * s + n, n)
        return remote(kv.at[src], kv.at[src], kvs.at[s], kvr.at[s], lax.rem(e + 2 * s, n), t)

    def kv_mate(s):
        src = lax.rem(e - 2 * s + n, n)
        return remote(kv.at[src], kv.at[src], kvs.at[half + s], kvr.at[half + s], mate, t)

    def kv_mate_in(s):
        src = lax.rem(mate - 2 * s + n, n)
        return remote(kv.at[src], kv.at[src], kvs.at[half + s], kvr.at[half + s], mate, t)

    def source(s):
        s = jnp.int32(s)
        flipped = jnp.int32(0)
        bit = 1
        while bit < n:
            ours = lax.rem(lax.div(e, jnp.int32(bit)), jnp.int32(2))
            theirs = lax.rem(lax.div(s, jnp.int32(bit)), jnp.int32(2))
            flipped = flipped + bit * (ours + theirs - 2 * ours * theirs)
            bit *= 2
        return flipped

    def send_a(s):
        dst = source(s)
        return remote(sbuf.at[dst], recv.at[e, t], a_s.at[s], a_r.at[s], dst, t)

    def send_near(s):
        dst = source(s)
        return remote(sbuf2.at[dst], recv.at[e, peer], bx_s.at[s], bx_r.at[s], dst, t)

    def copy_a(s):
        src = source(s)
        return remote(sbuf.at[src], recv.at[src, t], a_s.at[s], a_r.at[s], src, t)

    def copy_bx(s, col):
        src = source(s)
        return remote(recv.at[src, col], recv.at[src, col], bx_s.at[s], bx_r.at[s], e, peer)

    def copy_bc(s, col):
        src = source(s)
        return remote(recv.at[src, col], recv.at[src, col], bc_s.at[s], bc_r.at[s], e, partner)

    def copy_c(s, col):
        src = source(s)
        return remote(recv.at[src, col], recv.at[src, col], c_s.at[s], c_r.at[s], e, partner)

    def copy_r1(s, which, col):
        src = source(s)
        return remote(
            part.at[src, col], r1.at[src, which], r1_s.at[s, which], r1_r.at[s, which], e, partner
        )

    def copy_r2(s):
        src = source(s)
        return remote(s2.at[src], r2.at[src], r2_s.at[s], r2_r.at[s], e, peer)

    def copy_r3(s):
        src = source(s)
        return remote(s3.at[src], rbuf.at[e], r3_s.at[s], r3_r.at[s], src, t)

    def copy_r3_in(s):
        src = source(s)
        return remote(s3.at[src], rbuf.at[src], r3_s.at[s], r3_r.at[s], src, t)

    pl.semaphore_wait(barrier, n - 1 + tpn - 1)

    lanes = 2 * n * cap
    place = lax.broadcasted_iota(jnp.int32, (own_rows, lanes), 1).astype(jnp.float32) + 0.5
    expert = jnp.floor(place / (2.0 * cap))
    inside = place - 0.5 - expert * (2.0 * cap)
    right = inside >= cap
    slot = jnp.where(right, inside - cap, inside)
    top, share = routes_ref.shape

    def column(line, j):
        at = lax.rem(t + j, tpn) * own_rows
        own = lax.broadcasted_iota(jnp.int32, (own_rows, share), 1) == (
            lax.broadcasted_iota(jnp.int32, (own_rows, share), 0) + at
        )
        return jnp.sum(
            jnp.where(own, jnp.broadcast_to(line, own.shape), 0.0), axis=1, keepdims=True
        )

    def route(k, j):
        return column(routes_ref[k : k + 1, :].astype(jnp.float32), j)

    before = lax.broadcasted_iota(jnp.int32, (own_rows, own_rows), 1) < lax.broadcasted_iota(
        jnp.int32, (own_rows, own_rows), 0
    )

    def choose(j):
        named = [route(k, j) == expert for k in range(top)]
        total = sum([m.astype(jnp.float32) for m in named])
        rank = jnp.dot(
            before.astype(jnp.bfloat16),
            total.astype(jnp.bfloat16),
            preferred_element_type=jnp.float32,
        )
        hit = rank == slot
        chosen = jnp.where(hit, total, 0.0)
        spread = jnp.concatenate(
            [jnp.where(right, 0.0, chosen), jnp.where(right, chosen, 0.0)], axis=0
        )
        return spread.T.astype(jnp.bfloat16), hit, named

    load_r.wait()
    spread, hit, named = choose(0)
    load_n.wait()
    gain = gain_ref[...].astype(jnp.float32)
    gain = jnp.concatenate([gain[j : j + 1, :] for j in range(gain.shape[0])], axis=1)

    def halves(j):
        load_x(j).wait()
        x = xbuf[j].astype(jnp.float32)
        scale = lax.rsqrt(jnp.mean(x * x, axis=-1, keepdims=True) + 1e-06)
        normed = (x * scale * gain).astype(jnp.bfloat16)
        return jnp.concatenate([normed[:, :wide], normed[:, wide:]], axis=0)

    stacked = halves(0)
    outgoing = jnp.dot(spread, stacked, preferred_element_type=jnp.float32)
    sbuf[...] = outgoing.astype(jnp.bfloat16).reshape(sbuf.shape)
    for s in range(half, n):
        send_a(s).start()
    for s in range(1, half):
        send_a(s).start()
    keep = pltpu.make_async_copy(sbuf.at[e], recv.at[e, t], lsem.at[7])
    keep.start()
    outgoing = jnp.dot(choose(2)[0], halves(2), preferred_element_type=jnp.float32)
    sbuf2[...] = outgoing.astype(jnp.bfloat16).reshape(sbuf2.shape)
    for s in range(1, half):
        send_near(s).start()
    recv[e, peer] = sbuf2[e]
    keep.wait()
    for k in range(top):
        mine = jnp.where(hit & named[k], 1.0, 0.0)
        sel[2 * k * own_rows : (2 * k + 1) * own_rows, :] = jnp.where(right, 0.0, mine).astype(
            jnp.bfloat16
        )
        sel[(2 * k + 1) * own_rows : (2 * k + 2) * own_rows, :] = jnp.where(
            right, mine, 0.0
        ).astype(jnp.bfloat16)
    load_k.wait()
    load_v.wait()
    for s in range(1, half):
        kv_far(s).start()
    kv_mate(0).start()

    lane = lax.broadcasted_iota(jnp.int32, (own_rows, 2 * cap), 1)
    lane_right = lane >= cap
    lane_slot = jnp.where(lane_right, lane - cap, lane).astype(jnp.float32)
    mine_expert = e.astype(jnp.float32)
    for j in (1, 3):
        hits = sum(
            [jnp.where(route(k, j) == mine_expert, 1.0, 0.0) for k in range(top)]
        )
        hits = jnp.broadcast_to(hits, lane.shape)
        ranks = jnp.dot(
            before.astype(jnp.bfloat16),
            hits.astype(jnp.bfloat16),
            preferred_element_type=jnp.float32,
        )
        here = jnp.where(ranks == lane_slot, hits, 0.0)
        here = jnp.concatenate(
            [jnp.where(lane_right, 0.0, here), jnp.where(lane_right, here, 0.0)], axis=0
        )
        recv[e, lax.rem(t + j, tpn)] = jnp.dot(
            here.T.astype(jnp.bfloat16), halves(j), preferred_element_type=jnp.float32
        ).astype(jnp.bfloat16)

    def copy_att(s):
        dst = lax.rem(t + s, tpn)
        return remote(att.at[dst], attr.at[t], ats.at[s], atr.at[s], e, dst)

    def copy_att_in(s):
        src = lax.rem(t - s + tpn, tpn)
        return remote(att.at[src], attr.at[src], ats.at[s], atr.at[s], e, lax.rem(t + s, tpn))

    def attention():
        for s in range(half):
            kv_mate_in(s).wait_recv()
        load_q.wait()
        load_c.wait()
        own_gate = gate_ref[:, pl.ds(pl.multiple_of(e * seq, seq), seq)]
        eye = lax.broadcasted_iota(jnp.int32, (seq, seq), 0) == lax.broadcasted_iota(
            jnp.int32, (seq, seq), 1
        )
        gate_col = jnp.sum(
            jnp.where(eye, jnp.broadcast_to(own_gate, (seq, seq)), 0.0), axis=1, keepdims=True
        )
        key_pos = lax.broadcasted_iota(jnp.int32, (seq, n * seq), 1)
        query_pos = lax.broadcasted_iota(jnp.int32, (seq, n * seq), 0) + e * seq
        bias = gate_col - gate_ref[...]
        group = q_ref.shape[1] // head
        heads_out = []
        for g in range(group):
            q = q_ref[:, g * head : (g + 1) * head]
            scores = jnp.concatenate(
                [
                    jnp.dot(q, kv[j, 0:head, :], preferred_element_type=jnp.float32)
                    for j in range(n)
                ],
                axis=1,
            )
            scores = scores * (head ** (-0.5)) + bias
            scores = jnp.where(key_pos <= query_pos, scores, -jnp.inf)
            weights = jnp.exp(scores - jnp.max(scores, axis=-1, keepdims=True))
            whole = jnp.sum(weights, axis=-1, keepdims=True)
            weights = weights.astype(jnp.bfloat16)
            summed = jnp.zeros((seq, head), jnp.float32)
            for j in range(n):
                summed = summed + lax.dot_general(
                    weights[:, j * seq : (j + 1) * seq],
                    kv[j, head : 2 * head, :],
                    (((1,), (1,)), ((), ())),
                    preferred_element_type=jnp.float32,
                )
            heads_out.append(summed / whole)
        attended = jnp.concatenate(heads_out, axis=1).astype(jnp.bfloat16)
        att[...] = attended.reshape(att.shape)
        attr[t] = att[t]
        for s in range(1, tpn):
            copy_att(s).start()

    load_g.wait()
    load_u.wait()
    load_d.wait()

    def order(p):
        skip = lax.div(p, jnp.int32(half + 1))
        later = lax.div(p + n - 1, jnp.int32(n))
        return later * lax.rem(p + half - 1 + skip, n)

    def step(i, carry):
        @pl.when(i == n - 2)
        def _():
            for s in range(1, half):
                kv_far_in(s).wait_recv()
                kv_mate(s).start()

        @pl.when(i == n)
        def _():
            attention()

        @pl.when(i < n)
        def _():
            s = order(i)

            @pl.when(s > 0)
            def _():
                copy_a(s).wait_recv()

                @pl.when(s >= half)
                def _():
                    copy_bx(s, t).start()

                copy_bc(s, t).start()

        @pl.when((i >= 1) & (i <= n))
        def _():
            s = order(i - 1)

            @pl.when(s > 0)
            def _():
                copy_bx(s, peer).wait_recv()
                copy_c(s, peer).start()

        @pl.when((i >= 2) & (i <= n + 1))
        def _():
            s = order(i - 2)
            src = source(s)

            @pl.when(s > 0)
            def _():
                copy_bc(s, partner).wait_recv()
                copy_c(s, opp).wait_recv()

            block = recv[src].astype(jnp.float32)
            count = block.shape[0] * cap
            lo = block[:, :cap].reshape(count, wide).astype(jnp.bfloat16)
            hi = block[:, cap:].reshape(count, wide).astype(jnp.bfloat16)
            gate = jnp.dot(lo, wgv[0:wide, :], preferred_element_type=jnp.float32) + jnp.dot(
                hi, wgv[wide:, :], preferred_element_type=jnp.float32
            )
            upper = jnp.dot(lo, wuv[0:wide, :], preferred_element_type=jnp.float32) + jnp.dot(
                hi, wuv[wide:, :], preferred_element_type=jnp.float32
            )
            hidden = (gate / (1.0 + jnp.exp(-gate)) * upper).astype(jnp.bfloat16)
            down = jnp.dot(hidden, wdv[...], preferred_element_type=jnp.float32)
            shape = (tpn, cap, wide)
            part[src] = jnp.concatenate(
                [down[:, :wide].reshape(shape), down[:, wide:].reshape(shape)], axis=1
            ).astype(jnp.bfloat16)
            copy_r1(s, 1, opp).start()
            copy_r1(s, 0, partner).start()

        @pl.when((i >= 3) & (i <= n + 2))
        def _():
            s = order(i - 3)
            src = source(s)
            copy_r1(s, 1, opp).wait_recv()
            copy_r1(s, 0, partner).wait_recv()
            s2[src] = (
                part[src, peer].astype(jnp.float32) + r1[src, 1].astype(jnp.float32)
            ).astype(jnp.bfloat16)
            copy_r2(s).start()

        @pl.when(i >= 4)
        def _():
            s = order(i - 4)
            src = source(s)
            copy_r2(s).wait_recv()
            s3[src] = (
                part[src, t].astype(jnp.float32)
                + r1[src, 0].astype(jnp.float32)
                + r2[src].astype(jnp.float32)
            ).astype(jnp.bfloat16)

            @pl.when(s > 0)
            def _():
                copy_r3(s).start()

            @pl.when(s == 0)
            def _():
                rbuf[e] = s3[e]

        return carry

    lax.fori_loop(0, n + 4, step, 0)

    for s in range(1, tpn):
        copy_att_in(s).wait_recv()
    load_o.wait()
    joined = jnp.concatenate([attr[j] for j in range(tpn)], axis=1)
    mixed_ref[...] = jnp.dot(joined, owv[...], preferred_element_type=jnp.float32).astype(
        jnp.bfloat16
    )

    for s in range(1, n):
        copy_r3_in(s).wait_recv()
    picked = jnp.dot(
        sel[...], rbuf[...].reshape(lanes, wide), preferred_element_type=jnp.float32
    )
    load_w.wait()
    rw = [column(rw_ref[k : k + 1, :], 0) for k in range(top)]
    for h in range(2):
        acc = jnp.zeros((own_rows, wide), jnp.float32)
        for k in range(top):
            at = (2 * k + h) * own_rows
            acc = acc + rw[k] * picked[at : at + own_rows]
        out_ref[:, h * wide : (h + 1) * wide] = acc.astype(jnp.bfloat16)

    for s in range(1, half):
        kv_far(s).wait_send()
    for s in range(half):
        kv_mate(s).wait_send()
    for s in range(1, tpn):
        copy_att(s).wait_send()

    def drain(s, carry):
        copy_r1(s, 0, partner).wait_send()
        copy_r1(s, 1, opp).wait_send()
        copy_r2(s).wait_send()

        @pl.when(s > 0)
        def _():
            send_a(s).wait_send()
            copy_bx(s, t).wait_send()
            copy_bc(s, t).wait_send()
            copy_c(s, peer).wait_send()
            copy_r3(s).wait_send()

        return carry

    lax.fori_loop(0, n, drain, 0)


def fused_body(
    n,
    tpn,
    queries,
    key_cache,
    value_cache,
    cum_gate,
    out_weight,
    routed_input,
    norm_gain,
    routes,
    route_weight,
    expert_gate,
    expert_up,
    expert_down,
):
    seq = queries.shape[0]
    head = key_cache.shape[1]
    width = routed_input.shape[1]
    wide = width // 2
    own_rows = routed_input.shape[0] // tpn
    top = routes.shape[1]
    units = expert_gate.shape[2]
    cap = block_capacity(own_rows, top, n * expert_gate.shape[0])
    bf16 = jnp.bfloat16
    chunk = (2 * cap, wide)
    vmem = pl.BlockSpec(memory_space=pltpu.VMEM)
    anywhere = pl.BlockSpec(memory_space=pltpu.HBM)
    dma = pltpu.SemaphoreType.DMA
    mixed, out = pl.pallas_call(
        functools.partial(fused_kernel, n, tpn, cap),
        out_shape=(
            jax.ShapeDtypeStruct((seq // tpn, width), bf16),
            jax.ShapeDtypeStruct((own_rows, width), bf16),
        ),
        in_specs=[anywhere] * 12,
        out_specs=(vmem, vmem),
        scratch_shapes=[
            pltpu.VMEM(queries.shape, bf16),
            pltpu.VMEM(cum_gate.shape, jnp.float32),
            pltpu.VMEM((width // 128, 128), bf16),
            pltpu.VMEM((top, tpn * own_rows), jnp.int32),
            pltpu.VMEM((top, tpn * own_rows), jnp.float32),
            pltpu.VMEM((tpn, own_rows, width), bf16),
            pltpu.VMEM((width, units), bf16),
            pltpu.VMEM((width, units), bf16),
            pltpu.VMEM((units, width), bf16),
            pltpu.VMEM(out_weight.shape, bf16),
            pltpu.VMEM((n, 2 * head, seq), bf16),
            pltpu.VMEM((tpn, seq // tpn, queries.shape[1]), bf16),
            pltpu.VMEM((tpn, seq // tpn, queries.shape[1]), bf16),
            pltpu.VMEM((2 * top * own_rows, 2 * n * cap), bf16),
            pltpu.VMEM((n,) + chunk, bf16),
            pltpu.VMEM((n,) + chunk, bf16),
            pltpu.VMEM((n, tpn) + chunk, bf16),
            pltpu.VMEM((n, tpn) + chunk, bf16),
            pltpu.VMEM((n, 2) + chunk, bf16),
            pltpu.VMEM((n,) + chunk, bf16),
            pltpu.VMEM((n,) + chunk, bf16),
            pltpu.VMEM((n,) + chunk, bf16),
            pltpu.VMEM((n,) + chunk, bf16),
            dma((12 + tpn,)),
            dma((n,)),
            dma((n,)),
            dma((tpn,)),
            dma((tpn,)),
        ]
        + [dma((n,))] * 8
        + [dma((n, 2))] * 2
        + [dma((n,))] * 4,
        compiler_params=pltpu.CompilerParams(
            collective_id=0, has_side_effects=True, vmem_limit_bytes=60 * 1024 * 1024
        ),
    )(
        queries,
        cum_gate,
        norm_gain.reshape(width // 128, 128),
        routes.T,
        route_weight.T,
        key_cache,
        value_cache,
        out_weight,
        routed_input,
        expert_gate,
        expert_up,
        expert_down,
    )
    return mixed, out


def block_capacity(own_rows, top_count, expert_count):
    return max(2, own_rows * top_count * 3 // (2 * expert_count))


def slot_chooser(route_rows, expert_count, capacity):
    token_rows, top_count = route_rows.shape
    flat = route_rows.reshape(token_rows * top_count)
    same = (flat[:, None] == jnp.arange(expert_count, dtype=jnp.int32)[None, :]).astype(jnp.int32)
    earlier = jnp.cumsum(same, axis=0) - same
    rank = jnp.sum(earlier * same, axis=1)
    slot = flat * capacity + rank
    chosen = slot[:, None] == jnp.arange(expert_count * capacity, dtype=jnp.int32)[None, :]
    return chosen.astype(jnp.bfloat16).reshape(token_rows, top_count, expert_count * capacity)


def rms_rows(source, norm_gain):
    widened = source.astype(jnp.float32)
    scale = lax.rsqrt(jnp.mean(widened * widened, axis=-1, keepdims=True) + 1e-06)
    return (widened * scale * norm_gain.astype(jnp.float32)).astype(jnp.bfloat16)


def mixer_half(queries, key_cache, value_cache, cum_gate, out_weight):
    seq_rows = queries.shape[0]
    local_heads = key_cache.shape[0]
    head_size = key_cache.shape[1]
    group = queries.shape[1] // (local_heads * head_size)
    own_start = lax.axis_index("ep") * seq_rows
    query_heads = queries.reshape(seq_rows, local_heads, group, head_size)
    query_pos = own_start + jnp.arange(seq_rows, dtype=jnp.int32)
    gate_query = lax.dynamic_slice_in_dim(cum_gate, own_start, seq_rows, 1)
    gate_rows = jnp.transpose(gate_query)[:, :, None, None]
    scale = head_size ** (-0.5)
    best_start = jnp.full((seq_rows, local_heads, group), -jnp.inf, jnp.float32)
    total_start = jnp.zeros((seq_rows, local_heads, group), jnp.float32)
    summed_start = jnp.zeros((seq_rows, local_heads * group * head_size), jnp.float32)
    pieces = (
        lax.all_gather(key_cache, "ep", axis=2, tiled=True),
        lax.all_gather(value_cache, "ep", axis=2, tiled=True),
    )

    def update(state):
        best, total, summed = state
        key_piece, value_piece = pieces
        width = key_piece.shape[2]
        scores = (
            jnp.einsum("thgd,hds->thgs", query_heads, key_piece, preferred_element_type=jnp.float32)
            * scale
        )
        scores = scores + gate_rows - cum_gate[None, :, None, :]
        key_pos = jnp.arange(width, dtype=jnp.int32)
        allowed = key_pos[None, :] <= query_pos[:, None]
        scores = jnp.where(allowed[:, None, None, :], scores, -jnp.inf)
        new_best = jnp.max(scores, axis=-1)
        factor = jnp.exp(best - new_best)
        weights = jnp.exp(scores - new_best[..., None])
        new_total = total * factor + jnp.sum(weights, axis=-1)
        product = jnp.einsum(
            "thgs,hds->thgd",
            weights.astype(jnp.bfloat16),
            value_piece,
            preferred_element_type=jnp.float32,
        )
        new_summed = summed.reshape(product.shape) * factor[..., None] + product
        return (new_best, new_total, new_summed.reshape(seq_rows, local_heads * group * head_size))

    best, total, summed = lax.cond(
        jnp.int32(0) <= own_start,
        update,
        lambda state: state,
        (best_start, total_start, summed_start),
    )
    attended = summed.reshape(seq_rows, local_heads, group, head_size) / total[..., None]
    attended = attended.astype(jnp.bfloat16).reshape(seq_rows, local_heads * group * head_size)
    by_position = lax.all_to_all(attended, "tp", split_axis=0, concat_axis=1, tiled=True)
    return jnp.dot(by_position, out_weight, preferred_element_type=jnp.float32).astype(jnp.bfloat16)


def expert_half(routed_input, norm_gain, routes, route_weight, expert_gate, expert_up, expert_down):
    group_size = lax.axis_size("tp")
    ep_size = lax.axis_size("ep")
    tp_index = lax.axis_index("tp")
    seq_rows, width = routed_input.shape
    own_rows = seq_rows // group_size
    local_experts = expert_gate.shape[0]
    expert_count = local_experts * ep_size
    top_count = routes.shape[1]
    capacity = max(2, own_rows * top_count * 3 // (2 * expert_count))
    per_device = local_experts * capacity
    mine = lax.dynamic_slice_in_dim(routed_input, tp_index * own_rows, own_rows, 0)
    own_routes = lax.dynamic_slice_in_dim(routes, tp_index * own_rows, own_rows, 0)
    chooser = slot_chooser(own_routes, expert_count, capacity)
    normed = rms_rows(mine, norm_gain)
    outgoing = jnp.einsum("tks,td->sd", chooser, normed, preferred_element_type=jnp.float32).astype(
        jnp.bfloat16
    )
    arrived = lax.all_to_all(
        outgoing.reshape(1, ep_size, per_device, width),
        "ep",
        split_axis=1,
        concat_axis=1,
        tiled=True,
    )
    received = lax.all_gather(arrived, "tp", axis=0, tiled=True)
    blocks = received.shape[0]
    divide_point = received.reshape(blocks, ep_size, local_experts, capacity, width)
    gate = jnp.einsum(
        "abecd,edf->abecf", divide_point, expert_gate, preferred_element_type=jnp.float32
    )
    upper = jnp.einsum(
        "abecd,edf->abecf", divide_point, expert_up, preferred_element_type=jnp.float32
    )
    hidden = (jax.nn.silu(gate) * upper).astype(jnp.bfloat16)
    partial_value = jnp.einsum(
        "abecf,efd->abecd", hidden, expert_down, preferred_element_type=jnp.float32
    )
    rounded = lax.optimization_barrier(partial_value.astype(jnp.bfloat16)).astype(jnp.float32)
    summed = lax.psum_scatter(
        rounded.reshape(lax.axis_size("tp") * 1, ep_size, per_device, width).astype(jnp.bfloat16),
        "tp",
        scatter_dimension=0,
        tiled=True,
    )
    returned = lax.all_to_all(summed, "ep", split_axis=1, concat_axis=1, tiled=True)
    picked = jnp.einsum(
        "tks,sd->tkd",
        chooser,
        returned.reshape(ep_size * per_device, width),
        preferred_element_type=jnp.float32,
    )
    own_weight = lax.dynamic_slice_in_dim(route_weight, tp_index * own_rows, own_rows, 0)
    return jnp.sum(own_weight[:, :, None] * picked, axis=1).astype(jnp.bfloat16)


def body(
    queries,
    key_cache,
    value_cache,
    cum_gate,
    out_weight,
    routed_input,
    norm_gain,
    routes,
    route_weight,
    expert_gate,
    expert_up,
    expert_down,
):
    mixed_out = mixer_half(queries, key_cache, value_cache, cum_gate, out_weight)
    expert_out = expert_half(
        routed_input, norm_gain, routes, route_weight, expert_gate, expert_up, expert_down
    )
    return (mixed_out, expert_out)


def pick_body(
    n,
    tpn,
    queries,
    key_cache,
    value_cache,
    cum_gate,
    out_weight,
    routed_input,
    norm_gain,
    routes,
    route_weight,
    expert_gate,
    *rest,
):
    seq, columns = queries.shape
    own_rows = routed_input.shape[0] // tpn
    cap = block_capacity(own_rows, routes.shape[1], n * expert_gate.shape[0])
    fits = (
        tpn == 4
        and n >= 4
        and n & (n - 1) == 0
        and cap % 8 == 0
        and expert_gate.shape[0] == 1
        and key_cache.shape[0] == 1
        and seq % 128 == 0
    )
    args = (
        queries,
        key_cache,
        value_cache,
        cum_gate,
        out_weight,
        routed_input,
        norm_gain,
        routes,
        route_weight,
        expert_gate,
    ) + rest
    return fused_body(n, tpn, *args) if fits else body(*args)


def solution(mesh):
    return jax.shard_map(
        functools.partial(pick_body, mesh.shape["ep"], mesh.shape["tp"]),
        mesh=mesh,
        in_specs=(
            P("ep", "tp"),
            P("tp", None, "ep"),
            P("tp", None, "ep"),
            P("tp", None),
            P(),
            P("ep", None),
            P(),
            P("ep", None),
            P("ep", None),
            P("ep", None, "tp"),
            P("ep", None, "tp"),
            P("ep", "tp", None),
        ),
        out_specs=(P(("ep", "tp"), None), P(("ep", "tp"), None)),
        check_vma=False,
    )
```

profile of v0, /device:TPU:8, one launch (start us, length us, event | category | flops | bytes accessed | tf_op | source)
XLA Modules:
  0.0 59.7 jit_solution(5988424667385391330)
XLA Ops:
  0.6 55.8 %shard_map.131 = (bf16[32,2048]{1,0:T(8,128)(2,1)}, bf16[64,2048]{1,0:T(8,128)(2,1)}) custom-call(bf16[128,128]{1,0:T(8,128)(2,1)} %q_any.1, f32[1,1024]{1,0:T(1,128)} %gate_any.1, bf16[16,128]{1,0:T(8,128)(2,1)} %bitcast.3, s32[2,256]{1,0:T(2,128)} %bitcast.4, f32[2,256]{1,0:T(2,128)} %bitcast.5, bf16[1,64,128]{2,1,0:T(8,128)(2,1)} %k_any.1, ...), custom_call_target="tpu_custom_call" | custom-call | tf_op jit(solution)/shard_map/pallas_call | solution.py:545
  56.4 1.6 %copy.16 = bf16[32,2048]{1,0:T(8,128)(2,1)} copy(bf16[32,2048]{1,0:T(8,128)(2,1)} %get-tuple-element.4) | data formatting | bytes 262144
  58.0 1.7 %copy.17 = bf16[64,2048]{1,0:T(8,128)(2,1)} copy(bf16[64,2048]{1,0:T(8,128)(2,1)} %get-tuple-element.5) | data formatting | bytes 524288
where the time goes:
time: 59.8 us; the launch traced here: 59.7 us
  Pallas kernels  55.8 us (93%)
  local copies, waits for them, and re-layouts  3.24 us (5%)
  between operations  0.64 us (1%)
    pallas_call x1, Pallas kernels, fused_body(): pl.pallas_call(functools.partial(fused_kernel, n, tpn, cap), out_shape=(j...  55.8 us
    unnamed x2, local copies, waits for them, and re-layouts  3.24 us

commit v1 on v0

--- a/solution.py
+++ b/solution.py
@@ -8,6 +8,21 @@
 from jax.sharding import PartitionSpec as P
 
 MESH = pl.DeviceIdType.MESH
+
+
+INNER_SENDS = (1, 3, 2)
+OUTER_SENDS = (3, 1, 2)
+LAND_SENDS = (3, 1, 2)
+INNER_STEPS = (
+    "C0", "D0", "E0", "A1", "L1", "A6", "C1", "D1", "L0", "A7", "B6", "K", "C6", "A4",
+    "A2", "A3", "E1", "D6", "B7", "C7", "B4", "D7", "A5", "C3", "E6", "C4", "T", "E7",
+    "D4", "D3", "C2", "B5", "C5", "D2", "E4", "E3", "D5", "E2", "E5",
+)
+OUTER_STEPS = (
+    "C0", "D0", "A3", "E0", "C3", "A1", "A2", "D3", "C1", "A7", "C2", "A6", "E3", "B7",
+    "A5", "A4", "C7", "B6", "D7", "C6", "B5", "K", "D6", "D2", "E7", "C5", "B4", "C4",
+    "D5", "D1", "E6", "D4", "E5", "E2", "T", "E1", "E4",
+)
 
 
 def fused_kernel(
@@ -42,8 +57,11 @@
     att,
     attr,
     sel,
+    raw,
+    land,
+    lroutes,
     sbuf,
-    sbuf2,
+    sland,
     recv,
     part,
     r1,
@@ -56,14 +74,15 @@
     kvr,
     ats,
     atr,
+    w_s,
+    w_r,
     a_s,
     a_r,
+    l_s,
     bx_s,
     bx_r,
-    bc_s,
-    bc_r,
-    c_s,
-    c_r,
+    f_s,
+    f_r,
     r1_s,
     r1_r,
     r2_s,
@@ -83,6 +102,13 @@
     head = k_any.shape[1]
     seq = q_ref.shape[0]
 
+    side = lax.div(e, half)
+    base = side * half
+    local = lax.rem(e, half)
+    row = lax.rem(e, 2)
+    inner = lax.div(local, 2) == 1 - side
+    rank = jnp.where(inner, 0, 1)
+
     barrier = pltpu.get_barrier_semaphore()
     for s in range(1, n):
         pl.semaphore_signal(
@@ -93,8 +119,10 @@
             barrier, inc=1, device_id={"ep": e, "tp": lax.rem(t + s, tpn)}, device_id_type=MESH
         )
 
+    blocks = (t, peer, partner, opp)
+
     def load_x(j):
-        at = lax.rem(t + j, tpn) * own_rows
+        at = blocks[j] * own_rows
         return pltpu.make_async_copy(x_any.at[pl.ds(at, own_rows)], xbuf.at[j], lsem.at[12 + j])
 
     load_k = pltpu.make_async_copy(k_any.at[0], kv.at[e, pl.ds(0, head)], lsem.at[1])
@@ -108,19 +136,20 @@
     load_n = pltpu.make_async_copy(gain_any, gain_ref, lsem.at[10])
     load_r = pltpu.make_async_copy(routes_any, routes_ref, lsem.at[11])
     load_w = pltpu.make_async_copy(rw_any, rw_ref, lsem.at[0])
+    load_r.start()
+    load_n.start()
+    load_x(0).start()
+    load_x(1).start()
     load_k.start()
     load_v.start()
-    load_x(0).start()
-    load_r.start()
-    load_n.start()
-    load_w.start()
-    load_q.start()
-    load_c.start()
-    for j in range(1, tpn):
+    for j in range(2, tpn):
         load_x(j).start()
     load_g.start()
     load_u.start()
     load_d.start()
+    load_w.start()
+    load_q.start()
+    load_c.start()
     load_o.start()
 
     def remote(src, dst, ssem, rsem, ep, tp):
@@ -133,22 +162,7 @@
             device_id_type=MESH,
         )
 
-    def kv_far(s):
-        return remote(kv.at[e], kv.at[e], kvs.at[s], kvr.at[s], lax.rem(e + 2 * s, n), t)
-
-    def kv_far_in(s):
-        src = lax.rem(e - 2 * s + n, n)
-        return remote(kv.at[src], kv.at[src], kvs.at[s], kvr.at[s], lax.rem(e + 2 * s, n), t)
-
-    def kv_mate(s):
-        src = lax.rem(e - 2 * s + n, n)
-        return remote(kv.at[src], kv.at[src], kvs.at[half + s], kvr.at[half + s], mate, t)
-
-    def kv_mate_in(s):
-        src = lax.rem(mate - 2 * s + n, n)
-        return remote(kv.at[src], kv.at[src], kvs.at[half + s], kvr.at[half + s], mate, t)
-
-    def source(s):
+    def flip(s):
         s = jnp.int32(s)
         flipped = jnp.int32(0)
         bit = 1
@@ -159,60 +173,101 @@
             bit *= 2
         return flipped
 
-    def send_a(s):
-        dst = source(s)
-        return remote(sbuf.at[dst], recv.at[e, t], a_s.at[s], a_r.at[s], dst, t)
-
-    def send_near(s):
-        dst = source(s)
-        return remote(sbuf2.at[dst], recv.at[e, peer], bx_s.at[s], bx_r.at[s], dst, t)
-
-    def copy_a(s):
-        src = source(s)
-        return remote(sbuf.at[src], recv.at[src, t], a_s.at[s], a_r.at[s], src, t)
-
-    def copy_bx(s, col):
-        src = source(s)
-        return remote(recv.at[src, col], recv.at[src, col], bx_s.at[s], bx_r.at[s], e, peer)
-
-    def copy_bc(s, col):
-        src = source(s)
-        return remote(recv.at[src, col], recv.at[src, col], bc_s.at[s], bc_r.at[s], e, partner)
-
-    def copy_c(s, col):
-        src = source(s)
-        return remote(recv.at[src, col], recv.at[src, col], c_s.at[s], c_r.at[s], e, partner)
-
-    def copy_r1(s, which, col):
-        src = source(s)
+    def kv_far(s):
+        return remote(kv.at[e], kv.at[e], kvs.at[s], kvr.at[s], lax.rem(e + 2 * s, n), t)
+
+    def kv_far_in(s):
+        src = lax.rem(e - 2 * s + n, n)
+        return remote(kv.at[src], kv.at[src], kvs.at[s], kvr.at[s], lax.rem(e + 2 * s, n), t)
+
+    def kv_mate(s):
+        src = lax.rem(e - 2 * s + n, n)
+        return remote(kv.at[src], kv.at[src], kvs.at[half + s], kvr.at[half + s], mate, t)
+
+    def kv_mate_in(s):
+        src = lax.rem(mate - 2 * s + n, n)
+        return remote(kv.at[src], kv.at[src], kvs.at[half + s], kvr.at[half + s], mate, t)
+
+    def far_sends(s):
+        return e + 2 * s < n
+
+    def far_comes(s):
+        return e - 2 * s >= 0
+
+    def mate_sends(s):
+        return (e - 2 * s >= 0) if s else row == 0
+
+    def mate_comes(s):
+        return (mate - 2 * s >= 0) if s else row == 1
+
+    across = (2 - side) * 2 + row
+    send_raw = remote(raw, land.at[rank], w_s.at[0], w_r.at[rank], across, t)
+    send_routes = remote(routes_ref, lroutes.at[rank], w_s.at[1], w_r.at[2 + rank], across, t)
+
+    def raw_in(j):
+        return remote(raw, land.at[j], w_s.at[0], w_r.at[j], across, t)
+
+    def routes_in(j):
+        return remote(routes_ref, lroutes.at[j], w_s.at[1], w_r.at[2 + j], across, t)
+
+    def near(s):
+        dst = flip(s)
         return remote(
-            part.at[src, col], r1.at[src, which], r1_s.at[s, which], r1_r.at[s, which], e, partner
-        )
-
-    def copy_r2(s):
-        src = source(s)
-        return remote(s2.at[src], r2.at[src], r2_s.at[s], r2_r.at[s], e, peer)
-
-    def copy_r3(s):
-        src = source(s)
-        return remote(s3.at[src], rbuf.at[e], r3_s.at[s], r3_r.at[s], src, t)
+            sbuf.at[lax.rem(dst, half)],
+            recv.at[s, pl.ds(0, 2)],
+            a_s.at[s],
+            a_r.at[s],
+            dst,
+            t,
+        )
+
+    def landed(j, s):
+        dst = flip(s)
+        return remote(
+            sland.at[j, lax.rem(dst, half)],
+            recv.at[half + 2 * j + s % 2, 0],
+            l_s.at[j, s],
+            a_r.at[half + 2 * j + s % 2],
+            dst,
+            t,
+        )
+
+    def landed_in(g):
+        return remote(sland.at[0, 0], recv.at[g, 0], l_s.at[0, 0], a_r.at[g], e, peer)
+
+    def copy_bx(g):
+        return remote(recv.at[g, 0], recv.at[g, 1], bx_s.at[g], bx_r.at[g], e, peer)
+
+    def copy_f(g):
+        return remote(
+            recv.at[g, pl.ds(0, 2)], recv.at[g, pl.ds(2, 2)], f_s.at[g], f_r.at[g], e, partner
+        )
+
+    def copy_r1(g):
+        return remote(part.at[g, pl.ds(2, 2)], r1.at[g], r1_s.at[g], r1_r.at[g], e, partner)
+
+    def copy_r2(g):
+        return remote(s2.at[g], r2.at[g], r2_s.at[g], r2_r.at[g], e, peer)
+
+    def source(g):
+        g = jnp.int32(g)
+        which = lax.div(g - half, jnp.int32(2))
+        turn = lax.rem(g, jnp.int32(2))
+        z = jnp.where(side == 0, 2 + which, 1 - which)
+        far = 2 * z + row + turn - 2 * row * turn
+        return jnp.where(g < half, flip(g), far)
+
+    def copy_r3(g):
+        return remote(s3.at[g], rbuf.at[e], r3_s.at[g], r3_r.at[e], source(g), t)
 
     def copy_r3_in(s):
-        src = source(s)
-        return remote(s3.at[src], rbuf.at[src], r3_s.at[s], r3_r.at[s], src, t)
-
-    pl.semaphore_wait(barrier, n - 1 + tpn - 1)
-
-    lanes = 2 * n * cap
-    place = lax.broadcasted_iota(jnp.int32, (own_rows, lanes), 1).astype(jnp.float32) + 0.5
-    expert = jnp.floor(place / (2.0 * cap))
-    inside = place - 0.5 - expert * (2.0 * cap)
-    right = inside >= cap
-    slot = jnp.where(right, inside - cap, inside)
+        src = flip(s)
+        return remote(s3.at[0], rbuf.at[src], r3_s.at[0], r3_r.at[src], src, t)
+
     top, share = routes_ref.shape
 
-    def column(line, j):
-        at = lax.rem(t + j, tpn) * own_rows
+    def column(line, block):
+        at = block * own_rows
         own = lax.broadcasted_iota(jnp.int32, (own_rows, share), 1) == (
             lax.broadcasted_iota(jnp.int32, (own_rows, share), 0) + at
         )
@@ -220,30 +275,49 @@
             jnp.where(own, jnp.broadcast_to(line, own.shape), 0.0), axis=1, keepdims=True
         )
 
-    def route(k, j):
-        return column(routes_ref[k : k + 1, :].astype(jnp.float32), j)
+    def named_by(ref, block):
+        return [column(ref[k : k + 1, :].astype(jnp.float32), block) for k in range(top)]
 
     before = lax.broadcasted_iota(jnp.int32, (own_rows, own_rows), 1) < lax.broadcasted_iota(
         jnp.int32, (own_rows, own_rows), 0
     )
 
-    def choose(j):
-        named = [route(k, j) == expert for k in range(top)]
+    def lanes_of(first, count):
+        lanes = 2 * count * cap
+        place = lax.broadcasted_iota(jnp.int32, (own_rows, lanes), 1).astype(jnp.float32) + 0.5
+        expert = jnp.floor(place / (2.0 * cap))
+        inside = place - 0.5 - expert * (2.0 * cap)
+        right = inside >= cap
+        slot = jnp.where(right, inside - cap, inside)
+        return expert + first.astype(jnp.float32), right, slot
+
+    def hits_of(names, lanes):
+        expert, right, slot = lanes
+        named = [name == expert for name in names]
         total = sum([m.astype(jnp.float32) for m in named])
-        rank = jnp.dot(
+        ranks = jnp.dot(
             before.astype(jnp.bfloat16),
             total.astype(jnp.bfloat16),
             preferred_element_type=jnp.float32,
         )
-        hit = rank == slot
+        return named, total, ranks == slot
+
+    def spread_of(names, lanes):
+        _, total, hit = hits_of(names, lanes)
+        right = lanes[1]
         chosen = jnp.where(hit, total, 0.0)
         spread = jnp.concatenate(
             [jnp.where(right, 0.0, chosen), jnp.where(right, chosen, 0.0)], axis=0
         )
-        return spread.T.astype(jnp.bfloat16), hit, named
+        return spread.T.astype(jnp.bfloat16)
+
+    def chunks(spread, rows):
+        return jnp.dot(spread, rows, preferred_element_type=jnp.float32).astype(jnp.bfloat16)
 
     load_r.wait()
-    spread, hit, named = choose(0)
+    side_lanes = lanes_of(base, half)
+    own_names = named_by(routes_ref, t)
+    spread = spread_of(own_names, side_lanes)
     load_n.wait()
     gain = gain_ref[...].astype(jnp.float32)
     gain = jnp.concatenate([gain[j : j + 1, :] for j in range(gain.shape[0])], axis=1)
@@ -255,56 +329,43 @@
         normed = (x * scale * gain).astype(jnp.bfloat16)
         return jnp.concatenate([normed[:, :wide], normed[:, wide:]], axis=0)
 
-    stacked = halves(0)
-    outgoing = jnp.dot(spread, stacked, preferred_element_type=jnp.float32)
-    sbuf[...] = outgoing.astype(jnp.bfloat16).reshape(sbuf.shape)
-    for s in range(half, n):
-        send_a(s).start()
-    for s in range(1, half):
-        send_a(s).start()
-    keep = pltpu.make_async_copy(sbuf.at[e], recv.at[e, t], lsem.at[7])
-    keep.start()
-    outgoing = jnp.dot(choose(2)[0], halves(2), preferred_element_type=jnp.float32)
-    sbuf2[...] = outgoing.astype(jnp.bfloat16).reshape(sbuf2.shape)
-    for s in range(1, half):
-        send_near(s).start()
-    recv[e, peer] = sbuf2[e]
-    keep.wait()
-    for k in range(top):
-        mine = jnp.where(hit & named[k], 1.0, 0.0)
-        sel[2 * k * own_rows : (2 * k + 1) * own_rows, :] = jnp.where(right, 0.0, mine).astype(
-            jnp.bfloat16
-        )
-        sel[(2 * k + 1) * own_rows : (2 * k + 2) * own_rows, :] = jnp.where(
-            right, mine, 0.0
-        ).astype(jnp.bfloat16)
+    own = halves(0)
+    raw[...] = own
+    sbuf[:, 0] = chunks(spread, own).reshape(half, 2 * cap, wide)
+
+    with jax.named_scope("barrier"):
+        pl.semaphore_wait(barrier, n - 1 + tpn - 1)
+    send_raw.start()
+    send_routes.start()
+    sbuf[:, 1] = chunks(spread_of(named_by(routes_ref, peer), side_lanes), halves(1)).reshape(
+        half, 2 * cap, wide
+    )
+    @pl.when(inner)
+    def _():
+        for s in INNER_SENDS:
+            near(s).start()
+
+    @pl.when(jnp.logical_not(inner))
+    def _():
+        for s in OUTER_SENDS:
+            near(s).start()
+
     load_k.wait()
     load_v.wait()
     for s in range(1, half):
-        kv_far(s).start()
-    kv_mate(0).start()
-
-    lane = lax.broadcasted_iota(jnp.int32, (own_rows, 2 * cap), 1)
-    lane_right = lane >= cap
-    lane_slot = jnp.where(lane_right, lane - cap, lane).astype(jnp.float32)
-    mine_expert = e.astype(jnp.float32)
-    for j in (1, 3):
-        hits = sum(
-            [jnp.where(route(k, j) == mine_expert, 1.0, 0.0) for k in range(top)]
-        )
-        hits = jnp.broadcast_to(hits, lane.shape)
-        ranks = jnp.dot(
-            before.astype(jnp.bfloat16),
-            hits.astype(jnp.bfloat16),
-            preferred_element_type=jnp.float32,
-        )
-        here = jnp.where(ranks == lane_slot, hits, 0.0)
-        here = jnp.concatenate(
-            [jnp.where(lane_right, 0.0, here), jnp.where(lane_right, here, 0.0)], axis=0
-        )
-        recv[e, lax.rem(t + j, tpn)] = jnp.dot(
-            here.T.astype(jnp.bfloat16), halves(j), preferred_element_type=jnp.float32
-        ).astype(jnp.bfloat16)
+
+        @pl.when(far_sends(s))
+        def _():
+            kv_far(s).start()
+
+    @pl.when(mate_sends(0))
+    def _():
+        kv_mate(0).start()
+
+    own_lanes = lanes_of(e, 1)
+    recv[0, 0:2] = sbuf[local]
+    for j in (2, 3):
+        recv[0, j] = chunks(spread_of(named_by(routes_ref, blocks[j]), own_lanes), halves(j))
 
     def copy_att(s):
         dst = lax.rem(t + s, tpn)
@@ -316,7 +377,17 @@
 
     def attention():
         for s in range(half):
-            kv_mate_in(s).wait_recv()
+
+            @pl.when(mate_comes(s))
+            def _():
+                kv_mate_in(s).wait_recv()
+
+        for j in range(1, n):
+
+            @pl.when(j > e)
+            def _():
+                kv[j] = jnp.zeros(kv.shape[1:], kv.dtype)
+
         load_q.wait()
         load_c.wait()
         own_gate = gate_ref[:, pl.ds(pl.multiple_of(e * seq, seq), seq)]
@@ -360,127 +431,187 @@
         for s in range(1, tpn):
             copy_att(s).start()
 
-    load_g.wait()
-    load_u.wait()
-    load_d.wait()
-
-    def order(p):
-        skip = lax.div(p, jnp.int32(half + 1))
-        later = lax.div(p + n - 1, jnp.int32(n))
-        return later * lax.rem(p + half - 1 + skip, n)
-
-    def step(i, carry):
-        @pl.when(i == n - 2)
-        def _():
-            for s in range(1, half):
+    def pass_kv():
+        for s in range(1, half):
+
+            @pl.when(far_comes(s))
+            def _():
                 kv_far_in(s).wait_recv()
                 kv_mate(s).start()
 
-        @pl.when(i == n)
-        def _():
-            attention()
-
-        @pl.when(i < n)
-        def _():
-            s = order(i)
-
-            @pl.when(s > 0)
-            def _():
-                copy_a(s).wait_recv()
-
-                @pl.when(s >= half)
-                def _():
-                    copy_bx(s, t).start()
-
-                copy_bc(s, t).start()
-
-        @pl.when((i >= 1) & (i <= n))
-        def _():
-            s = order(i - 1)
-
-            @pl.when(s > 0)
-            def _():
-                copy_bx(s, peer).wait_recv()
-                copy_c(s, peer).start()
-
-        @pl.when((i >= 2) & (i <= n + 1))
-        def _():
-            s = order(i - 2)
-            src = source(s)
-
-            @pl.when(s > 0)
-            def _():
-                copy_bc(s, partner).wait_recv()
-                copy_c(s, opp).wait_recv()
-
-            block = recv[src].astype(jnp.float32)
-            count = block.shape[0] * cap
-            lo = block[:, :cap].reshape(count, wide).astype(jnp.bfloat16)
-            hi = block[:, cap:].reshape(count, wide).astype(jnp.bfloat16)
-            gate = jnp.dot(lo, wgv[0:wide, :], preferred_element_type=jnp.float32) + jnp.dot(
-                hi, wgv[wide:, :], preferred_element_type=jnp.float32
-            )
-            upper = jnp.dot(lo, wuv[0:wide, :], preferred_element_type=jnp.float32) + jnp.dot(
-                hi, wuv[wide:, :], preferred_element_type=jnp.float32
-            )
-            hidden = (gate / (1.0 + jnp.exp(-gate)) * upper).astype(jnp.bfloat16)
-            down = jnp.dot(hidden, wdv[...], preferred_element_type=jnp.float32)
-            shape = (tpn, cap, wide)
-            part[src] = jnp.concatenate(
-                [down[:, :wide].reshape(shape), down[:, wide:].reshape(shape)], axis=1
+    def land_rows(j):
+        with jax.named_scope(f"w_land{j}"):
+            raw_in(j).wait_recv()
+            routes_in(j).wait_recv()
+        names = named_by(lroutes.at[j], t)
+        sland[j] = chunks(spread_of(names, side_lanes), land[j]).reshape(half, 2 * cap, wide)
+        for s in LAND_SENDS:
+            landed(j, s).start()
+        recv[half + 2 * j, 0] = sland[j, local]
+
+    def arrive(g, here):
+        if g < half:
+            near_in(g).wait_recv()
+            copy_f(g).start()
+        else:
+            if not here or g % 2:
+                landed_in(g).wait_recv()
+            copy_bx(g).start()
+
+    def near_in(g):
+        return remote(
+            sbuf.at[0], recv.at[g, pl.ds(0, 2)], a_s.at[0], a_r.at[g], e, peer
+        )
+
+    def spread_pair(g):
+        copy_bx(g).wait_recv()
+        copy_f(g).start()
+
+    def experts(g):
+        if g:
+            with jax.named_scope(f"w_f{g}"):
+                copy_f(g).wait_recv()
+        block = recv[g].astype(jnp.float32)
+        count = block.shape[0] * cap
+        lo = block[:, :cap].reshape(count, wide).astype(jnp.bfloat16)
+        hi = block[:, cap:].reshape(count, wide).astype(jnp.bfloat16)
+        gate = jnp.dot(lo, wgv[0:wide, :], preferred_element_type=jnp.float32) + jnp.dot(
+            hi, wgv[wide:, :], preferred_element_type=jnp.float32
+        )
+        upper = jnp.dot(lo, wuv[0:wide, :], preferred_element_type=jnp.float32) + jnp.dot(
+            hi, wuv[wide:, :], preferred_element_type=jnp.float32
+        )
+        hidden = (gate / (1.0 + jnp.exp(-gate)) * upper).astype(jnp.bfloat16)
+        down = jnp.dot(hidden, wdv[...], preferred_element_type=jnp.float32)
+        shape = (tpn, cap, wide)
+        part[g] = jnp.concatenate(
+            [down[:, :wide].reshape(shape), down[:, wide:].reshape(shape)], axis=1
+        ).astype(jnp.bfloat16)
+        copy_r1(g).start()
+
+    def cross(g):
+        copy_r1(g).wait_recv()
+        s2[g] = (part[g, 1].astype(jnp.float32) + r1[g, 1].astype(jnp.float32)).astype(
+            jnp.bfloat16
+        )
+        copy_r2(g).start()
+
+    def give_back(g):
+        copy_r2(g).wait_recv()
+        done = (
+            part[g, 0].astype(jnp.float32)
+            + r1[g, 0].astype(jnp.float32)
+            + r2[g].astype(jnp.float32)
+        ).astype(jnp.bfloat16)
+        if g == 0:
+            rbuf[e] = done
+        else:
+            s3[g] = done
+            copy_r3(g).start()
+
+    def first_matmul():
+        load_g.wait()
+        load_u.wait()
+        load_d.wait()
+
+    def choose_back():
+        everywhere = lanes_of(e * 0, n)
+        named, _, hit = hits_of(own_names, everywhere)
+        right = everywhere[1]
+        for k in range(top):
+            mine = jnp.where(hit & named[k], 1.0, 0.0)
+            sel[2 * k * own_rows : (2 * k + 1) * own_rows, :] = jnp.where(
+                right, 0.0, mine
             ).astype(jnp.bfloat16)
-            copy_r1(s, 1, opp).start()
-            copy_r1(s, 0, partner).start()
-
-        @pl.when((i >= 3) & (i <= n + 2))
-        def _():
-            s = order(i - 3)
-            src = source(s)
-            copy_r1(s, 1, opp).wait_recv()
-            copy_r1(s, 0, partner).wait_recv()
-            s2[src] = (
-                part[src, peer].astype(jnp.float32) + r1[src, 1].astype(jnp.float32)
+            sel[(2 * k + 1) * own_rows : (2 * k + 2) * own_rows, :] = jnp.where(
+                right, mine, 0.0
             ).astype(jnp.bfloat16)
-            copy_r2(s).start()
-
-        @pl.when(i >= 4)
-        def _():
-            s = order(i - 4)
-            src = source(s)
-            copy_r2(s).wait_recv()
-            s3[src] = (
-                part[src, t].astype(jnp.float32)
-                + r1[src, 0].astype(jnp.float32)
-                + r2[src].astype(jnp.float32)
-            ).astype(jnp.bfloat16)
-
-            @pl.when(s > 0)
-            def _():
-                copy_r3(s).start()
-
-            @pl.when(s == 0)
-            def _():
-                rbuf[e] = s3[e]
-
-        return carry
-
-    lax.fori_loop(0, n + 4, step, 0)
-
-    for s in range(1, tpn):
-        copy_att_in(s).wait_recv()
-    load_o.wait()
+
+    def run(steps, here):
+        for name in steps:
+            kind = name[0]
+            with jax.named_scope(name):
+                if kind == "L":
+                    land_rows(int(name[1:]))
+                elif kind == "K":
+                    pass_kv()
+                elif kind == "T":
+                    attention()
+                elif kind == "A":
+                    arrive(int(name[1:]), here)
+                else:
+                    {"B": spread_pair, "C": experts, "D": cross, "E": give_back}[kind](
+                        int(name[1:])
+                    )
+
+    first_matmul()
+
+    @pl.when(inner)
+    def _():
+        run(INNER_STEPS, True)
+
+    @pl.when(jnp.logical_not(inner))
+    def _():
+        run(OUTER_STEPS, False)
+
+    choose_back()
+
+    with jax.named_scope("w_att"):
+        for s in range(1, tpn):
+            copy_att_in(s).wait_recv()
+        load_o.wait()
     joined = jnp.concatenate([attr[j] for j in range(tpn)], axis=1)
     mixed_ref[...] = jnp.dot(joined, owv[...], preferred_element_type=jnp.float32).astype(
         jnp.bfloat16
     )
-
-    for s in range(1, n):
-        copy_r3_in(s).wait_recv()
+    load_w.wait()
+    rw = [column(rw_ref[k : k + 1, :], t) for k in range(top)]
+
+    send_raw.wait_send()
+    send_routes.wait_send()
+    for s in range(1, half):
+        near(s).wait_send()
+
+        @pl.when(far_sends(s))
+        def _():
+            kv_far(s).wait_send()
+
+        @pl.when(inner)
+        def _():
+            for j in range(2):
+                landed(j, s).wait_send()
+
+    for s in range(half):
+
+        @pl.when(mate_sends(s))
+        def _():
+            kv_mate(s).wait_send()
+
+    for s in range(1, tpn):
+        copy_att(s).wait_send()
+
+    def drain(g, carry):
+        @pl.when(g > 0)
+        def _():
+            copy_f(g).wait_send()
+
+        @pl.when(g >= half)
+        def _():
+            copy_bx(g).wait_send()
+
+        copy_r1(g).wait_send()
+        copy_r2(g).wait_send()
+        return carry
+
+    lax.fori_loop(0, n, drain, 0)
+
+    with jax.named_scope("w_r3"):
+        for s in range(1, n):
+            copy_r3_in(s).wait_recv()
+    lanes = 2 * n * cap
     picked = jnp.dot(
         sel[...], rbuf[...].reshape(lanes, wide), preferred_element_type=jnp.float32
     )
-    load_w.wait()
-    rw = [column(rw_ref[k : k + 1, :], 0) for k in range(top)]
     for h in range(2):
         acc = jnp.zeros((own_rows, wide), jnp.float32)
         for k in range(top):
@@ -488,29 +619,11 @@
             acc = acc + rw[k] * picked[at : at + own_rows]
         out_ref[:, h * wide : (h + 1) * wide] = acc.astype(jnp.bfloat16)
 
-    for s in range(1, half):
-        kv_far(s).wait_send()
-    for s in range(half):
-        kv_mate(s).wait_send()
-    for s in range(1, tpn):
-        copy_att(s).wait_send()
-
-    def drain(s, carry):
-        copy_r1(s, 0, partner).wait_send()
-        copy_r1(s, 1, opp).wait_send()
-        copy_r2(s).wait_send()
-
-        @pl.when(s > 0)
-        def _():
-            send_a(s).wait_send()
-            copy_bx(s, t).wait_send()
-            copy_bc(s, t).wait_send()
-            copy_c(s, peer).wait_send()
-            copy_r3(s).wait_send()
-
+    def last(g, carry):
+        copy_r3(g).wait_send()
         return carry
 
-    lax.fori_loop(0, n, drain, 0)
+    lax.fori_loop(1, n, last, 0)
 
 
 def fused_body(
@@ -537,16 +650,17 @@
     top = routes.shape[1]
     units = expert_gate.shape[2]
     cap = block_capacity(own_rows, top, n * expert_gate.shape[0])
+    half = n // 2
     bf16 = jnp.bfloat16
     chunk = (2 * cap, wide)
+    anywhere = pl.BlockSpec(memory_space=pltpu.HBM)
     vmem = pl.BlockSpec(memory_space=pltpu.VMEM)
-    anywhere = pl.BlockSpec(memory_space=pltpu.HBM)
     dma = pltpu.SemaphoreType.DMA
     mixed, out = pl.pallas_call(
         functools.partial(fused_kernel, n, tpn, cap),
         out_shape=(
-            jax.ShapeDtypeStruct((seq // tpn, width), bf16),
-            jax.ShapeDtypeStruct((own_rows, width), bf16),
+            pltpu.VMEM((seq // tpn, width), bf16),
+            pltpu.VMEM((own_rows, width), bf16),
         ),
         in_specs=[anywhere] * 12,
         out_specs=(vmem, vmem),
@@ -565,8 +679,11 @@
             pltpu.VMEM((tpn, seq // tpn, queries.shape[1]), bf16),
             pltpu.VMEM((tpn, seq // tpn, queries.shape[1]), bf16),
             pltpu.VMEM((2 * top * own_rows, 2 * n * cap), bf16),
-            pltpu.VMEM((n,) + chunk, bf16),
-            pltpu.VMEM((n,) + chunk, bf16),
+            pltpu.VMEM((2 * own_rows, wide), bf16),
+            pltpu.VMEM((2, 2 * own_rows, wide), bf16),
+            pltpu.VMEM((2, top, tpn * own_rows), jnp.int32),
+            pltpu.VMEM((half, 2) + chunk, bf16),
+            pltpu.VMEM((2, half) + chunk, bf16),
             pltpu.VMEM((n, tpn) + chunk, bf16),
             pltpu.VMEM((n, tpn) + chunk, bf16),
             pltpu.VMEM((n, 2) + chunk, bf16),
@@ -579,10 +696,13 @@
             dma((n,)),
             dma((tpn,)),
             dma((tpn,)),
+            dma((2,)),
+            dma((4,)),
+            dma((half,)),
+            dma((n,)),
+            dma((2, half)),
         ]
-        + [dma((n,))] * 8
-        + [dma((n, 2))] * 2
-        + [dma((n,))] * 4,
+        + [dma((n,))] * 10,
         compiler_params=pltpu.CompilerParams(
             collective_id=0, has_side_effects=True, vmem_limit_bytes=60 * 1024 * 1024
         ),
@@ -600,7 +720,28 @@
         expert_up,
         expert_down,
     )
-    return mixed, out
+    return write_out(mixed, out)
+
+
+def write_kernel(a, b, a_out, b_out, sem):
+    copies = [
+        pltpu.make_async_copy(a, a_out, sem.at[0]),
+        pltpu.make_async_copy(b, b_out, sem.at[1]),
+    ]
+    for copy in copies:
+        copy.start()
+    for copy in copies:
+        copy.wait()
+
+
+def write_out(*arrays):
+    return pl.pallas_call(
+        write_kernel,
+        out_shape=[jax.ShapeDtypeStruct(a.shape, a.dtype) for a in arrays],
+        in_specs=[pl.BlockSpec(memory_space=pltpu.VMEM)] * len(arrays),
+        out_specs=[pl.BlockSpec(memory_space=pltpu.HBM)] * len(arrays),
+        scratch_shapes=[pltpu.SemaphoreType.DMA((len(arrays),))],
+    )(*[pltpu.with_memory_space_constraint(a, pltpu.VMEM) for a in arrays])
 
 
 def block_capacity(own_rows, top_count, expert_count):
@@ -777,8 +918,7 @@
     cap = block_capacity(own_rows, routes.shape[1], n * expert_gate.shape[0])
     fits = (
         tpn == 4
-        and n >= 4
-        and n & (n - 1) == 0
+        and n == 8
         and cap % 8 == 0
         and expert_gate.shape[0] == 1
         and key_cache.shape[0] == 1

time: 59.8 us -> 52.4 us (0.88)
  Pallas kernels: 55.8 us -> 51.5 us
  local copies, waits for them, and re-layouts: 3.24 us -> 0 us
    pallas_call x1 -> x2, Pallas kernels: 55.8 us -> 51.5 us  [the longest x1 50.8 us: fused_body(): pl.pallas_call(functools.partial(fused_kernel, n, tpn, cap), out_shape=(p...]
    unnamed x2 -> x0, local copies, waits for them, and re-layouts: 3.24 us -> none
where the time goes in v1:
time: 52.4 us; the launch traced here: 52.2 us
  Pallas kernels  51.5 us (98%)
  between operations  0.64 us (1%)
    pallas_call x1, Pallas kernels, fused_body(): pl.pallas_call(functools.partial(fused_kernel, n, tpn, cap), out_shape=(p...  50.8 us

profile of v1, /device:TPU:8, one launch (start us, length us, event | category | flops | bytes accessed | tf_op | source)
XLA Modules:
  0.0 52.2 jit_solution(4986284027187979197)
XLA Ops:
  0.6 50.8 %shard_map.131 = (bf16[32,2048]{1,0:T(8,128)(2,1)S(1)}, bf16[64,2048]{1,0:T(8,128)(2,1)S(1)}) custom-call(bf16[128,128]{1,0:T(8,128)(2,1)} %q_any.1, f32[1,1024]{1,0:T(1,128)} %gate_any.1, bf16[16,128]{1,0:T(8,128)(2,1)} %bitcast.3, s32[2,256]{1,0:T(2,128)} %bitcast.4, f32[2,256]{1,0:T(2,128)} %bitcast.5, bf16[1,64,128]{2,1,0:T(8,128)(2,1)} %k_any.1, ...), custom_call_target="tpu_custom_call" | custom-call | tf_op jit(solution)/shard_map/pallas_call | solution.py:659
  51.4 0.8 %shard_map.132 = (bf16[32,2048]{1,0:T(8,128)(2,1)}, bf16[64,2048]{1,0:T(8,128)(2,1)}) custom-call(bf16[32,2048]{1,0:T(8,128)(2,1)S(1)} %get-tuple-element.4.a, bf16[64,2048]{1,0:T(8,128)(2,1)S(1)} %get-tuple-element.5.b), custom_call_target="tpu_custom_call" | custom-call | tf_op jit(solution)/shard_map/pallas_call | solution.py:738

commit v2 on v1

--- a/solution.py
+++ b/solution.py
@@ -10,18 +10,17 @@
 MESH = pl.DeviceIdType.MESH
 
 
-INNER_SENDS = (1, 3, 2)
-OUTER_SENDS = (3, 1, 2)
-LAND_SENDS = (3, 1, 2)
+INNER_SENDS = (2, 7, 1, 5, 4, 6, 3)
+OUTER_SENDS = (7, 1, 4, 2, 6, 5, 3)
 INNER_STEPS = (
-    "C0", "D0", "E0", "A1", "L1", "A6", "C1", "D1", "L0", "A7", "B6", "K", "C6", "A4",
-    "A2", "A3", "E1", "D6", "B7", "C7", "B4", "D7", "A5", "C3", "E6", "C4", "T", "E7",
-    "D4", "D3", "C2", "B5", "C5", "D2", "E4", "E3", "D5", "E2", "E5",
+    "C0", "A1", "A6", "C1", "D1", "B6", "A2", "A5", "C6", "E1", "D6", "B5", "C2", "A7",
+    "A4", "E6", "C5", "A3", "D5", "C3", "B7", "B4", "D3", "C7", "K", "D7", "C4", "D2",
+    "E5", "E3", "D4", "E7", "D0", "T", "E2", "E4", "E0",
 )
 OUTER_STEPS = (
-    "C0", "D0", "A3", "E0", "C3", "A1", "A2", "D3", "C1", "A7", "C2", "A6", "E3", "B7",
-    "A5", "A4", "C7", "B6", "D7", "C6", "B5", "K", "D6", "D2", "E7", "C5", "B4", "C4",
-    "D5", "D1", "E6", "D4", "E5", "E2", "T", "E1", "E4",
+    "C0", "D0", "A7", "E0", "B7", "A5", "A2", "C7", "A1", "B5", "A6", "D7", "C5", "D5",
+    "C1", "B6", "A4", "C6", "E7", "K", "D6", "A3", "E5", "C3", "D1", "B4", "D3", "E6",
+    "C2", "C4", "D4", "D2", "E3", "T", "E1", "E4", "E2",
 )
 
 
@@ -57,11 +56,8 @@
     att,
     attr,
     sel,
-    raw,
-    land,
-    lroutes,
     sbuf,
-    sland,
+    sfar,
     recv,
     part,
     r1,
@@ -74,11 +70,8 @@
     kvr,
     ats,
     atr,
-    w_s,
-    w_r,
     a_s,
     a_r,
-    l_s,
     bx_s,
     bx_r,
     f_s,
@@ -200,16 +193,6 @@
     def mate_comes(s):
         return (mate - 2 * s >= 0) if s else row == 1
 
-    across = (2 - side) * 2 + row
-    send_raw = remote(raw, land.at[rank], w_s.at[0], w_r.at[rank], across, t)
-    send_routes = remote(routes_ref, lroutes.at[rank], w_s.at[1], w_r.at[2 + rank], across, t)
-
-    def raw_in(j):
-        return remote(raw, land.at[j], w_s.at[0], w_r.at[j], across, t)
-
-    def routes_in(j):
-        return remote(routes_ref, lroutes.at[j], w_s.at[1], w_r.at[2 + j], across, t)
-
     def near(s):
         dst = flip(s)
         return remote(
@@ -221,19 +204,17 @@
             t,
         )
 
-    def landed(j, s):
-        dst = flip(s)
+    def far(g):
+        dst = source(g)
+        mine = half + 2 * rank + g % 2
         return remote(
-            sland.at[j, lax.rem(dst, half)],
-            recv.at[half + 2 * j + s % 2, 0],
-            l_s.at[j, s],
-            a_r.at[half + 2 * j + s % 2],
-            dst,
-            t,
-        )
-
-    def landed_in(g):
-        return remote(sland.at[0, 0], recv.at[g, 0], l_s.at[0, 0], a_r.at[g], e, peer)
+            sfar.at[lax.rem(dst, half)], recv.at[mine, 0], a_s.at[g], a_r.at[mine], dst, t
+        )
+
+    def arrival(g):
+        if g < half:
+            return remote(sbuf.at[0], recv.at[g, pl.ds(0, 2)], a_s.at[0], a_r.at[g], e, peer)
+        return remote(sfar.at[0], recv.at[g, 0], a_s.at[0], a_r.at[g], e, peer)
 
     def copy_bx(g):
         return remote(recv.at[g, 0], recv.at[g, 1], bx_s.at[g], bx_r.at[g], e, peer)
@@ -330,26 +311,34 @@
         return jnp.concatenate([normed[:, :wide], normed[:, wide:]], axis=0)
 
     own = halves(0)
-    raw[...] = own
     sbuf[:, 0] = chunks(spread, own).reshape(half, 2 * cap, wide)
+    sfar[...] = chunks(spread_of(own_names, lanes_of(half - base, half)), own).reshape(sfar.shape)
 
     with jax.named_scope("barrier"):
         pl.semaphore_wait(barrier, n - 1 + tpn - 1)
-    send_raw.start()
-    send_routes.start()
+
+    def send(which):
+        for g in which:
+            (near if g < half else far)(g).start()
+
+    def leading(order):
+        return min(p for p, g in enumerate(order) if g < half)
+
+    def by_place(inner_part, outer_part):
+        @pl.when(inner)
+        def _():
+            send(inner_part)
+
+        @pl.when(jnp.logical_not(inner))
+        def _():
+            send(outer_part)
+
+    inner_first, outer_first = leading(INNER_SENDS), leading(OUTER_SENDS)
+    by_place(INNER_SENDS[:inner_first], OUTER_SENDS[:outer_first])
     sbuf[:, 1] = chunks(spread_of(named_by(routes_ref, peer), side_lanes), halves(1)).reshape(
         half, 2 * cap, wide
     )
-    @pl.when(inner)
-    def _():
-        for s in INNER_SENDS:
-            near(s).start()
-
-    @pl.when(jnp.logical_not(inner))
-    def _():
-        for s in OUTER_SENDS:
-            near(s).start()
-
+    by_place(INNER_SENDS[inner_first:], OUTER_SENDS[outer_first:])
     load_k.wait()
     load_v.wait()
     for s in range(1, half):
@@ -439,29 +428,9 @@
                 kv_far_in(s).wait_recv()
                 kv_mate(s).start()
 
-    def land_rows(j):
-        with jax.named_scope(f"w_land{j}"):
-            raw_in(j).wait_recv()
-            routes_in(j).wait_recv()
-        names = named_by(lroutes.at[j], t)
-        sland[j] = chunks(spread_of(names, side_lanes), land[j]).reshape(half, 2 * cap, wide)
-        for s in LAND_SENDS:
-            landed(j, s).start()
-        recv[half + 2 * j, 0] = sland[j, local]
-
-    def arrive(g, here):
-        if g < half:
-            near_in(g).wait_recv()
-            copy_f(g).start()
-        else:
-            if not here or g % 2:
-                landed_in(g).wait_recv()
-            copy_bx(g).start()
-
-    def near_in(g):
-        return remote(
-            sbuf.at[0], recv.at[g, pl.ds(0, 2)], a_s.at[0], a_r.at[g], e, peer
-        )
+    def arrive(g):
+        arrival(g).wait_recv()
+        (copy_f if g < half else copy_bx)(g).start()
 
     def spread_pair(g):
         copy_bx(g).wait_recv()
@@ -527,32 +496,27 @@
                 right, mine, 0.0
             ).astype(jnp.bfloat16)
 
-    def run(steps, here):
+    kinds = {"A": arrive, "B": spread_pair, "C": experts, "D": cross, "E": give_back}
+
+    def run(steps):
         for name in steps:
-            kind = name[0]
             with jax.named_scope(name):
-                if kind == "L":
-                    land_rows(int(name[1:]))
-                elif kind == "K":
+                if name == "K":
                     pass_kv()
-                elif kind == "T":
+                elif name == "T":
                     attention()
-                elif kind == "A":
-                    arrive(int(name[1:]), here)
                 else:
-                    {"B": spread_pair, "C": experts, "D": cross, "E": give_back}[kind](
-                        int(name[1:])
-                    )
+                    kinds[name[0]](int(name[1:]))
 
     first_matmul()
 
     @pl.when(inner)
     def _():
-        run(INNER_STEPS, True)
+        run(INNER_STEPS)
 
     @pl.when(jnp.logical_not(inner))
     def _():
-        run(OUTER_STEPS, False)
+        run(OUTER_STEPS)
 
     choose_back()
 
@@ -567,19 +531,13 @@
     load_w.wait()
     rw = [column(rw_ref[k : k + 1, :], t) for k in range(top)]
 
-    send_raw.wait_send()
-    send_routes.wait_send()
+    for g in range(1, n):
+        (near if g < half else far)(g).wait_send()
     for s in range(1, half):
-        near(s).wait_send()
 
         @pl.when(far_sends(s))
         def _():
             kv_far(s).wait_send()
-
-        @pl.when(inner)
-        def _():
-            for j in range(2):
-                landed(j, s).wait_send()
 
     for s in range(half):
 
@@ -679,11 +637,8 @@
             pltpu.VMEM((tpn, seq // tpn, queries.shape[1]), bf16),
             pltpu.VMEM((tpn, seq // tpn, queries.shape[1]), bf16),
             pltpu.VMEM((2 * top * own_rows, 2 * n * cap), bf16),
-            pltpu.VMEM((2 * own_rows, wide), bf16),
-            pltpu.VMEM((2, 2 * own_rows, wide), bf16),
-            pltpu.VMEM((2, top, tpn * own_rows), jnp.int32),
             pltpu.VMEM((half, 2) + chunk, bf16),
-            pltpu.VMEM((2, half) + chunk, bf16),
+            pltpu.VMEM((half,) + chunk, bf16),
             pltpu.VMEM((n, tpn) + chunk, bf16),
             pltpu.VMEM((n, tpn) + chunk, bf16),
             pltpu.VMEM((n, 2) + chunk, bf16),
@@ -696,13 +651,8 @@
             dma((n,)),
             dma((tpn,)),
             dma((tpn,)),
-            dma((2,)),
-            dma((4,)),
-            dma((half,)),
-            dma((n,)),
-            dma((2, half)),
         ]
-        + [dma((n,))] * 10,
+        + [dma((n,))] * 12,
         compiler_params=pltpu.CompilerParams(
             collective_id=0, has_side_effects=True, vmem_limit_bytes=60 * 1024 * 1024
         ),

time: 52.4 us -> 46.8 us (0.89)
  Pallas kernels: 51.5 us -> 46 us
    pallas_call x1, Pallas kernels: 50.8 us -> 45.2 us  [fused_body(): pl.pallas_call(functools.partial(fused_kernel, n, tpn, cap), out_shape=(p...]
where the time goes in v2:
time: 46.8 us; the launch traced here: 46.6 us
  Pallas kernels  46 us (98%)
  between operations  0.64 us (1%)
    pallas_call x1, Pallas kernels, fused_body(): pl.pallas_call(functools.partial(fused_kernel, n, tpn, cap), out_shape=(p...  45.2 us

profile of v2, /device:TPU:8, one launch (start us, length us, event | category | flops | bytes accessed | tf_op | source)
XLA Modules:
  0.0 46.6 jit_solution(1422139778891179586)
XLA Ops:
  0.6 45.2 %shard_map.131 = (bf16[32,2048]{1,0:T(8,128)(2,1)S(1)}, bf16[64,2048]{1,0:T(8,128)(2,1)S(1)}) custom-call(bf16[128,128]{1,0:T(8,128)(2,1)} %q_any.1, f32[1,1024]{1,0:T(1,128)} %gate_any.1, bf16[16,128]{1,0:T(8,128)(2,1)} %bitcast.3, s32[2,256]{1,0:T(2,128)} %bitcast.4, f32[2,256]{1,0:T(2,128)} %bitcast.5, bf16[1,64,128]{2,1,0:T(8,128)(2,1)} %k_any.1, ...), custom_call_target="tpu_custom_call" | custom-call | tf_op jit(solution)/shard_map/pallas_call | solution.py:617
  45.9 0.8 %shard_map.132 = (bf16[32,2048]{1,0:T(8,128)(2,1)}, bf16[64,2048]{1,0:T(8,128)(2,1)}) custom-call(bf16[32,2048]{1,0:T(8,128)(2,1)S(1)} %get-tuple-element.4.a, bf16[64,2048]{1,0:T(8,128)(2,1)S(1)} %get-tuple-element.5.b), custom_call_target="tpu_custom_call" | custom-call | tf_op jit(solution)/shard_map/pallas_call | solution.py:688

commit v3 on v2

--- a/solution.py
+++ b/solution.py
@@ -10,17 +10,17 @@
 MESH = pl.DeviceIdType.MESH
 
 
-INNER_SENDS = (2, 7, 1, 5, 4, 6, 3)
-OUTER_SENDS = (7, 1, 4, 2, 6, 5, 3)
+INNER_SENDS = (1, 2, 3, 6, 5, 7, 4)
+OUTER_SENDS = (4, 2, 7, 5, 1, 6, 3)
 INNER_STEPS = (
-    "C0", "A1", "A6", "C1", "D1", "B6", "A2", "A5", "C6", "E1", "D6", "B5", "C2", "A7",
-    "A4", "E6", "C5", "A3", "D5", "C3", "B7", "B4", "D3", "C7", "K", "D7", "C4", "D2",
-    "E5", "E3", "D4", "E7", "D0", "T", "E2", "E4", "E0",
+    "C0", "D0", "A6", "E0", "B6", "A2", "A5", "C2", "D2", "A7", "C6", "B5", "D6", "C5",
+    "D5", "E2", "B7", "C7", "E6", "A1", "A4", "A3", "C3", "E5", "D7", "C1", "D1", "B4",
+    "K", "D3", "C4", "E7", "D4", "E1", "E3", "E4", "T",
 )
 OUTER_STEPS = (
-    "C0", "D0", "A7", "E0", "B7", "A5", "A2", "C7", "A1", "B5", "A6", "D7", "C5", "D5",
-    "C1", "B6", "A4", "C6", "E7", "K", "D6", "A3", "E5", "C3", "D1", "B4", "D3", "E6",
-    "C2", "C4", "D4", "D2", "E3", "T", "E1", "E4", "E2",
+    "C0", "D0", "A4", "A1", "E0", "C1", "D1", "B4", "A7", "C4", "D4", "E1", "A6", "A2",
+    "B7", "E4", "A5", "C7", "A3", "C2", "D7", "B6", "C3", "D3", "K", "C6", "B5", "E7",
+    "D6", "C5", "E3", "D5", "E6", "D2", "T", "E5", "E2",
 )
 
 
@@ -68,20 +68,13 @@
     lsem,
     kvs,
     kvr,
-    ats,
-    atr,
-    a_s,
+    sent,
     a_r,
-    bx_s,
     bx_r,
-    f_s,
     f_r,
-    r1_s,
     r1_r,
-    r2_s,
     r2_r,
-    r3_s,
-    r3_r,
+    all_r,
 ):
     e = lax.axis_index("ep")
     t = lax.axis_index("tp")
@@ -198,7 +191,7 @@
         return remote(
             sbuf.at[lax.rem(dst, half)],
             recv.at[s, pl.ds(0, 2)],
-            a_s.at[s],
+            sent.at[0],
             a_r.at[s],
             dst,
             t,
@@ -208,27 +201,27 @@
         dst = source(g)
         mine = half + 2 * rank + g % 2
         return remote(
-            sfar.at[lax.rem(dst, half)], recv.at[mine, 0], a_s.at[g], a_r.at[mine], dst, t
+            sfar.at[lax.rem(dst, half)], recv.at[mine, 0], sent.at[0], a_r.at[mine], dst, t
         )
 
     def arrival(g):
         if g < half:
-            return remote(sbuf.at[0], recv.at[g, pl.ds(0, 2)], a_s.at[0], a_r.at[g], e, peer)
-        return remote(sfar.at[0], recv.at[g, 0], a_s.at[0], a_r.at[g], e, peer)
+            return remote(sbuf.at[0], recv.at[g, pl.ds(0, 2)], sent.at[0], a_r.at[g], e, peer)
+        return remote(sfar.at[0], recv.at[g, 0], sent.at[0], a_r.at[g], e, peer)
 
     def copy_bx(g):
-        return remote(recv.at[g, 0], recv.at[g, 1], bx_s.at[g], bx_r.at[g], e, peer)
+        return remote(recv.at[g, 0], recv.at[g, 1], sent.at[1], bx_r.at[g - half], e, peer)
 
     def copy_f(g):
         return remote(
-            recv.at[g, pl.ds(0, 2)], recv.at[g, pl.ds(2, 2)], f_s.at[g], f_r.at[g], e, partner
+            recv.at[g, pl.ds(0, 2)], recv.at[g, pl.ds(2, 2)], sent.at[2], f_r.at[g], e, partner
         )
 
     def copy_r1(g):
-        return remote(part.at[g, pl.ds(2, 2)], r1.at[g], r1_s.at[g], r1_r.at[g], e, partner)
+        return remote(part.at[g, pl.ds(2, 2)], r1.at[g], sent.at[3], r1_r.at[g], e, partner)
 
     def copy_r2(g):
-        return remote(s2.at[g], r2.at[g], r2_s.at[g], r2_r.at[g], e, peer)
+        return remote(s2.at[g], r2.at[g], sent.at[4], r2_r.at[g], e, peer)
 
     def source(g):
         g = jnp.int32(g)
@@ -239,11 +232,7 @@
         return jnp.where(g < half, flip(g), far)
 
     def copy_r3(g):
-        return remote(s3.at[g], rbuf.at[e], r3_s.at[g], r3_r.at[e], source(g), t)
-
-    def copy_r3_in(s):
-        src = flip(s)
-        return remote(s3.at[0], rbuf.at[src], r3_s.at[0], r3_r.at[src], src, t)
+        return remote(s3.at[g], rbuf.at[e], sent.at[5], all_r.at[0], source(g), t)
 
     top, share = routes_ref.shape
 
@@ -295,7 +284,8 @@
     def chunks(spread, rows):
         return jnp.dot(spread, rows, preferred_element_type=jnp.float32).astype(jnp.bfloat16)
 
-    load_r.wait()
+    with jax.named_scope("w_r"):
+        load_r.wait()
     side_lanes = lanes_of(base, half)
     own_names = named_by(routes_ref, t)
     spread = spread_of(own_names, side_lanes)
@@ -304,7 +294,8 @@
     gain = jnp.concatenate([gain[j : j + 1, :] for j in range(gain.shape[0])], axis=1)
 
     def halves(j):
-        load_x(j).wait()
+        with jax.named_scope(f"w_x{j}"):
+            load_x(j).wait()
         x = xbuf[j].astype(jnp.float32)
         scale = lax.rsqrt(jnp.mean(x * x, axis=-1, keepdims=True) + 1e-06)
         normed = (x * scale * gain).astype(jnp.bfloat16)
@@ -314,15 +305,16 @@
     sbuf[:, 0] = chunks(spread, own).reshape(half, 2 * cap, wide)
     sfar[...] = chunks(spread_of(own_names, lanes_of(half - base, half)), own).reshape(sfar.shape)
 
+    sbuf[:, 1] = chunks(spread_of(named_by(routes_ref, peer), side_lanes), halves(1)).reshape(
+        half, 2 * cap, wide
+    )
+
     with jax.named_scope("barrier"):
         pl.semaphore_wait(barrier, n - 1 + tpn - 1)
 
     def send(which):
         for g in which:
             (near if g < half else far)(g).start()
-
-    def leading(order):
-        return min(p for p, g in enumerate(order) if g < half)
 
     def by_place(inner_part, outer_part):
         @pl.when(inner)
@@ -333,12 +325,7 @@
         def _():
             send(outer_part)
 
-    inner_first, outer_first = leading(INNER_SENDS), leading(OUTER_SENDS)
-    by_place(INNER_SENDS[:inner_first], OUTER_SENDS[:outer_first])
-    sbuf[:, 1] = chunks(spread_of(named_by(routes_ref, peer), side_lanes), halves(1)).reshape(
-        half, 2 * cap, wide
-    )
-    by_place(INNER_SENDS[inner_first:], OUTER_SENDS[outer_first:])
+    by_place(INNER_SENDS, OUTER_SENDS)
     load_k.wait()
     load_v.wait()
     for s in range(1, half):
@@ -358,11 +345,12 @@
 
     def copy_att(s):
         dst = lax.rem(t + s, tpn)
-        return remote(att.at[dst], attr.at[t], ats.at[s], atr.at[s], e, dst)
-
-    def copy_att_in(s):
-        src = lax.rem(t - s + tpn, tpn)
-        return remote(att.at[src], attr.at[src], ats.at[s], atr.at[s], e, lax.rem(t + s, tpn))
+        return remote(att.at[dst], attr.at[t], sent.at[6], all_r.at[1], e, dst)
+
+    def joint(ref, ssem, rsem):
+        return remote(ref, ref, ssem, rsem, e, peer)
+
+    att_joint = joint(attr.at[pl.ds(0, tpn - 1)], sent.at[6], all_r.at[1])
 
     def attention():
         for s in range(half):
@@ -521,8 +509,7 @@
     choose_back()
 
     with jax.named_scope("w_att"):
-        for s in range(1, tpn):
-            copy_att_in(s).wait_recv()
+        att_joint.wait_recv()
         load_o.wait()
     joined = jnp.concatenate([attr[j] for j in range(tpn)], axis=1)
     mixed_ref[...] = jnp.dot(joined, owv[...], preferred_element_type=jnp.float32).astype(
@@ -531,8 +518,17 @@
     load_w.wait()
     rw = [column(rw_ref[k : k + 1, :], t) for k in range(top)]
 
-    for g in range(1, n):
-        (near if g < half else far)(g).wait_send()
+    fives = recv.at[pl.ds(0, half + 1), pl.ds(0, 2)]
+    for which, ref in enumerate(
+        (
+            fives,
+            recv.at[pl.ds(half, half), 0],
+            recv.at[pl.ds(1, n - 1), pl.ds(0, 2)],
+            part.at[:, pl.ds(2, 2)],
+            s2,
+        )
+    ):
+        joint(ref, sent.at[which], all_r.at[0]).wait_send()
     for s in range(1, half):
 
         @pl.when(far_sends(s))
@@ -545,27 +541,10 @@
         def _():
             kv_mate(s).wait_send()
 
-    for s in range(1, tpn):
-        copy_att(s).wait_send()
-
-    def drain(g, carry):
-        @pl.when(g > 0)
-        def _():
-            copy_f(g).wait_send()
-
-        @pl.when(g >= half)
-        def _():
-            copy_bx(g).wait_send()
-
-        copy_r1(g).wait_send()
-        copy_r2(g).wait_send()
-        return carry
-
-    lax.fori_loop(0, n, drain, 0)
+    att_joint.wait_send()
 
     with jax.named_scope("w_r3"):
-        for s in range(1, n):
-            copy_r3_in(s).wait_recv()
+        joint(rbuf.at[pl.ds(0, n - 1)], sent.at[5], all_r.at[0]).wait_recv()
     lanes = 2 * n * cap
     picked = jnp.dot(
         sel[...], rbuf[...].reshape(lanes, wide), preferred_element_type=jnp.float32
@@ -577,11 +556,7 @@
             acc = acc + rw[k] * picked[at : at + own_rows]
         out_ref[:, h * wide : (h + 1) * wide] = acc.astype(jnp.bfloat16)
 
-    def last(g, carry):
-        copy_r3(g).wait_send()
-        return carry
-
-    lax.fori_loop(1, n, last, 0)
+    joint(s3.at[pl.ds(1, n - 1)], sent.at[5], all_r.at[0]).wait_send()
 
 
 def fused_body(
@@ -649,10 +624,14 @@
             dma((12 + tpn,)),
             dma((n,)),
             dma((n,)),
-            dma((tpn,)),
-            dma((tpn,)),
-        ]
-        + [dma((n,))] * 12,
+            dma((7,)),
+            dma((n,)),
+            dma((half,)),
+            dma((n,)),
+            dma((n,)),
+            dma((n,)),
+            dma((2,)),
+        ],
         compiler_params=pltpu.CompilerParams(
             collective_id=0, has_side_effects=True, vmem_limit_bytes=60 * 1024 * 1024
         ),

time: 46.8 us -> 45.5 us (0.972)
  the two profiles are of different devices: /device:TPU:8 before, /device:TPU:0 now
where the time goes in v3:
time: 45.5 us; the launch traced here: 45.3 us
  Pallas kernels  44.7 us (98%)
  between operations  0.64 us (1%)
    pallas_call x1, Pallas kernels, fused_body(): pl.pallas_call(functools.partial(fused_kernel, n, tpn, cap), out_shape=(p...  43.9 us

profile of v3, /device:TPU:0, one launch (start us, length us, event | category | flops | bytes accessed | tf_op | source)
XLA Modules:
  0.0 45.3 jit_solution(17020077558022348828)
XLA Ops:
  0.6 43.9 %shard_map.131 = (bf16[32,2048]{1,0:T(8,128)(2,1)S(1)}, bf16[64,2048]{1,0:T(8,128)(2,1)S(1)}) custom-call(bf16[128,128]{1,0:T(8,128)(2,1)} %q_any.1, f32[1,1024]{1,0:T(1,128)} %gate_any.1, bf16[16,128]{1,0:T(8,128)(2,1)} %bitcast.3, s32[2,256]{1,0:T(2,128)} %bitcast.4, f32[2,256]{1,0:T(2,128)} %bitcast.5, bf16[1,64,128]{2,1,0:T(8,128)(2,1)} %k_any.1, ...), custom_call_target="tpu_custom_call" | custom-call | tf_op jit(solution)/shard_map/pallas_call | solution.py:592
  44.6 0.8 %shard_map.132 = (bf16[32,2048]{1,0:T(8,128)(2,1)}, bf16[64,2048]{1,0:T(8,128)(2,1)}) custom-call(bf16[32,2048]{1,0:T(8,128)(2,1)S(1)} %get-tuple-element.4.a, bf16[64,2048]{1,0:T(8,128)(2,1)S(1)} %get-tuple-element.5.b), custom_call_target="tpu_custom_call" | custom-call | tf_op jit(solution)/shard_map/pallas_call | solution.py:667

commit v4 on v3

--- a/solution.py
+++ b/solution.py
@@ -109,7 +109,7 @@
 
     def load_x(j):
         at = blocks[j] * own_rows
-        return pltpu.make_async_copy(x_any.at[pl.ds(at, own_rows)], xbuf.at[j], lsem.at[12 + j])
+        return pltpu.make_async_copy(x_any.at[pl.ds(at, own_rows)], xbuf.at[j], lsem.at[11 + j])
 
     load_k = pltpu.make_async_copy(k_any.at[0], kv.at[e, pl.ds(0, head)], lsem.at[1])
     load_v = pltpu.make_async_copy(v_any.at[0], kv.at[e, pl.ds(head, head)], lsem.at[2])
@@ -120,7 +120,7 @@
     load_q = pltpu.make_async_copy(q_any, q_ref, lsem.at[8])
     load_c = pltpu.make_async_copy(gate_any, gate_ref, lsem.at[9])
     load_n = pltpu.make_async_copy(gain_any, gain_ref, lsem.at[10])
-    load_r = pltpu.make_async_copy(routes_any, routes_ref, lsem.at[11])
+    load_r = pltpu.make_async_copy(routes_any, routes_ref, lsem.at[7])
     load_w = pltpu.make_async_copy(rw_any, rw_ref, lsem.at[0])
     load_r.start()
     load_n.start()
@@ -160,19 +160,19 @@
         return flipped
 
     def kv_far(s):
-        return remote(kv.at[e], kv.at[e], kvs.at[s], kvr.at[s], lax.rem(e + 2 * s, n), t)
+        return remote(kv.at[e], kv.at[e], kvs.at[s - 1], kvr.at[s - 1], lax.rem(e + 2 * s, n), t)
 
     def kv_far_in(s):
         src = lax.rem(e - 2 * s + n, n)
-        return remote(kv.at[src], kv.at[src], kvs.at[s], kvr.at[s], lax.rem(e + 2 * s, n), t)
+        return remote(kv.at[src], kv.at[src], kvs.at[s - 1], kvr.at[s - 1], lax.rem(e + 2 * s, n), t)
 
     def kv_mate(s):
         src = lax.rem(e - 2 * s + n, n)
-        return remote(kv.at[src], kv.at[src], kvs.at[half + s], kvr.at[half + s], mate, t)
+        return remote(kv.at[src], kv.at[src], kvs.at[half - 1 + s], kvr.at[half - 1 + s], mate, t)
 
     def kv_mate_in(s):
         src = lax.rem(mate - 2 * s + n, n)
-        return remote(kv.at[src], kv.at[src], kvs.at[half + s], kvr.at[half + s], mate, t)
+        return remote(kv.at[src], kv.at[src], kvs.at[half - 1 + s], kvr.at[half - 1 + s], mate, t)
 
     def far_sends(s):
         return e + 2 * s < n
@@ -192,7 +192,7 @@
             sbuf.at[lax.rem(dst, half)],
             recv.at[s, pl.ds(0, 2)],
             sent.at[0],
-            a_r.at[s],
+            a_r.at[s - 1],
             dst,
             t,
         )
@@ -201,20 +201,20 @@
         dst = source(g)
         mine = half + 2 * rank + g % 2
         return remote(
-            sfar.at[lax.rem(dst, half)], recv.at[mine, 0], sent.at[0], a_r.at[mine], dst, t
+            sfar.at[lax.rem(dst, half)], recv.at[mine, 0], sent.at[0], a_r.at[mine - 1], dst, t
         )
 
     def arrival(g):
         if g < half:
-            return remote(sbuf.at[0], recv.at[g, pl.ds(0, 2)], sent.at[0], a_r.at[g], e, peer)
-        return remote(sfar.at[0], recv.at[g, 0], sent.at[0], a_r.at[g], e, peer)
+            return remote(sbuf.at[0], recv.at[g, pl.ds(0, 2)], sent.at[0], a_r.at[g - 1], e, peer)
+        return remote(sfar.at[0], recv.at[g, 0], sent.at[0], a_r.at[g - 1], e, peer)
 
     def copy_bx(g):
         return remote(recv.at[g, 0], recv.at[g, 1], sent.at[1], bx_r.at[g - half], e, peer)
 
     def copy_f(g):
         return remote(
-            recv.at[g, pl.ds(0, 2)], recv.at[g, pl.ds(2, 2)], sent.at[2], f_r.at[g], e, partner
+            recv.at[g, pl.ds(0, 2)], recv.at[g, pl.ds(2, 2)], sent.at[2], f_r.at[g - 1], e, partner
         )
 
     def copy_r1(g):
@@ -621,13 +621,13 @@
             pltpu.VMEM((n,) + chunk, bf16),
             pltpu.VMEM((n,) + chunk, bf16),
             pltpu.VMEM((n,) + chunk, bf16),
-            dma((12 + tpn,)),
-            dma((n,)),
-            dma((n,)),
+            dma((11 + tpn,)),
+            dma((n - 1,)),
+            dma((n - 1,)),
             dma((7,)),
-            dma((n,)),
+            dma((n - 1,)),
             dma((half,)),
-            dma((n,)),
+            dma((n - 1,)),
             dma((n,)),
             dma((n,)),
             dma((2,)),

time: 45.5 us -> 45.4 us (level)
  no operation moved by 1% of the time
where the time goes in v4:
time: 45.4 us; the launch traced here: 45.3 us
  Pallas kernels  44.6 us (98%)
  between operations  0.64 us (1%)
    pallas_call x1, Pallas kernels, fused_body(): pl.pallas_call(functools.partial(fused_kernel, n, tpn, cap), out_shape=(p...  43.9 us

profile of v4, /device:TPU:0, one launch (start us, length us, event | category | flops | bytes accessed | tf_op | source)
XLA Modules:
  0.0 45.3 jit_solution(10941834558464952738)
XLA Ops:
  0.6 43.9 %shard_map.131 = (bf16[32,2048]{1,0:T(8,128)(2,1)S(1)}, bf16[64,2048]{1,0:T(8,128)(2,1)S(1)}) custom-call(bf16[128,128]{1,0:T(8,128)(2,1)} %q_any.1, f32[1,1024]{1,0:T(1,128)} %gate_any.1, bf16[16,128]{1,0:T(8,128)(2,1)} %bitcast.3, s32[2,256]{1,0:T(2,128)} %bitcast.4, f32[2,256]{1,0:T(2,128)} %bitcast.5, bf16[1,64,128]{2,1,0:T(8,128)(2,1)} %k_any.1, ...), custom_call_target="tpu_custom_call" | custom-call | tf_op jit(solution)/shard_map/pallas_call | solution.py:592
  44.5 0.8 %shard_map.132 = (bf16[32,2048]{1,0:T(8,128)(2,1)}, bf16[64,2048]{1,0:T(8,128)(2,1)}) custom-call(bf16[32,2048]{1,0:T(8,128)(2,1)S(1)} %get-tuple-element.4.a, bf16[64,2048]{1,0:T(8,128)(2,1)S(1)} %get-tuple-element.5.b), custom_call_target="tpu_custom_call" | custom-call | tf_op jit(solution)/shard_map/pallas_call | solution.py:667
